TPU v7x, 256 devices: a 4x2x16 block of a 4x16x16 slice. The times are simulated.
256 devices in a mesh: grp: 2 (over y), ep: 32 (over z, core), tp: 4 (over x).
Axes of the slice: x: 4, y: 2, z: 16, core: 2. Of those that a mesh axis runs over, the one named last changes fastest.
The devices are a block of a 4x16x16 slice.
Arguments:
- queries: bfloat16 [32768, 1024], P(('grp', 'ep'), 'tp'), parts along dimension 0, may hold values from -6 to 6
- key_rows: bfloat16 [32768, 512], P(('grp', 'ep'), 'tp'), parts along dimension 0, may hold values from -6 to 6
- value_rows: bfloat16 [32768, 512], P(('grp', 'ep'), 'tp'), parts along dimension 0, may hold values from -6 to 6
- query_gain: float32 [128], replicated, may hold values from 0.3 to 9
- key_gain: float32 [128], replicated, may hold values from 0.3 to 9
- log_forget: float32 [8, 32768], P('tp', 'grp'), parts along dimension 1, may hold values from -16384 to 0, as said below
- out_weight: bfloat16 [1024, 2048], P('tp'), may hold values from -0.1875 to 0.1875
- expert_rows: bfloat16 [32768, 2048], P(('grp', 'ep')), parts along dimension 0, may hold values from -6 to 6
- expert_gain: float32 [2048], replicated, may hold values from 0.1 to 1.9
- routes: int32 [2, 32768], P(None, ('grp', 'ep')), parts along dimension 1, may hold values from 0 to 31, as said below
- route_weight: float32 [2, 32768], P(None, ('grp', 'ep')), parts along dimension 1, may hold values from 0.1 to 1
- gate_weight: bfloat16 [32, 2048, 1024], P('ep', None, 'tp'), may hold values from -0.125 to 0.125
- up_weight: bfloat16 [32, 2048, 1024], P('ep', None, 'tp'), may hold values from -0.125 to 0.125
- down_weight: bfloat16 [32, 1024, 2048], P('ep', 'tp'), may hold values from -0.1875 to 0.1875
Outputs:
- mixer_out: bfloat16 [32768, 2048], P(('grp', 'ep', 'tp')), parts along dimension 0
- expert_out: bfloat16 [32768, 2048], P(('grp', 'ep'), 'tp'), parts along dimension 0
There are 2 independent parts, one for each index of `grp`. A program takes and returns all parts, laid end to end along the dimension named above; an argument that names none is the same for every part. Nothing has to cross between parts.
Inputs may be any that keep to these rules, and one draw needn't show every extreme that they name: `log_forget`: each head's values never rise along the positions. `routes`: the 2 experts of a token differ and lie in one group of 8 consecutive numbers. Among the tokens of one index of ep (512 consecutive tokens), no expert is named more than 48 times, and in every draw some experts are named exactly 48 times in every such block.
All inputs are finite; a program needn't handle non-finite values.
Results may differ from a plain program's by a relative error of at most 0.012.
The roundings to bfloat16 on the way count: a program that leaves them out, or rounds other values in their place, can miss the bound.
Values may be sent and summed in bfloat16 or wider, within the bound.
A program may use at most 128 MiB of HBM per device.

v0:
```python
import jax
import jax.numpy as jnp
from jax import lax
from jax.sharding import Mesh
from jax.sharding import PartitionSpec as P

HEAD_SIZE = 128
EXPERTS = 32
TOP = 2
EP = ("ep_0", "ep_1")
GRP_EP = ("grp", "ep_0", "ep_1")
GRP_EP_TP = ("grp", "ep_0", "ep_1", "tp")


def joined_along(parts, dim):
    parts = jnp.moveaxis(parts, 0, dim)
    shape = parts.shape
    return parts.reshape(*shape[:dim], shape[dim] * shape[dim + 1], *shape[dim + 2 :])


def stacked_from(value, axes, turns):
    parts = value[None]
    for k in turns:
        parts = lax.all_gather(parts, axes[k], axis=0, tiled=True)
    block = [lax.axis_size(axes[k]) for k in reversed(turns)]
    parts = parts.reshape(*block, *value.shape)
    turned = sorted(range(len(turns)), key=lambda place: turns[len(turns) - 1 - place])
    return parts.transpose(*turned, *range(len(turns), parts.ndim)).reshape(-1, *value.shape)


def gather_axes(value, axes, turns, dim):
    return joined_along(stacked_from(value, axes, turns), dim)


def in_blocks(value, dim, count):
    shape = value.shape
    parts = value.reshape(*shape[:dim], count, shape[dim] // count, *shape[dim + 1 :])
    return jnp.moveaxis(parts, dim, 0)


def turned_blocks(parts, axes, turns):
    shape = [lax.axis_size(a) for a in axes]
    parts = parts.reshape(*shape, *parts.shape[1:])
    for k in turns:
        parts = lax.all_to_all(parts, axes[k], split_axis=k, concat_axis=k, tiled=True)
    return parts.reshape(-1, *parts.shape[len(axes) :])


def core_and_chips(value, groups, turns, split_dim, concat_dim):
    count = lax.axis_size(groups[0]) * lax.axis_size(groups[1])
    parts = in_blocks(value, split_dim, count)
    return joined_along(turned_blocks(parts, groups, turns), concat_dim)


def head_norm(inputs, scale_gain):
    widened = inputs.astype(jnp.float32)
    factor = lax.rsqrt(jnp.mean(widened * widened, axis=-1, keepdims=True) + 1e-06)
    return widened * factor * scale_gain


def slot_table(chosen, experts_all, capacity):
    n_rows = chosen.shape[0]
    per_row = chosen.shape[1]
    flat_ids = chosen.reshape(-1)
    one_hot = (flat_ids[:, None] == jnp.arange(experts_all, dtype=jnp.int32)[None, :]).astype(
        jnp.int32
    )
    within = jnp.sum((jnp.cumsum(one_hot, axis=0) - 1) * one_hot, axis=1)
    slot_index = flat_ids * capacity + within
    row_of = jnp.arange(n_rows * per_row, dtype=jnp.int32) // per_row
    slot_owner = jnp.full((experts_all * capacity,), n_rows, jnp.int32).at[slot_index].set(row_of)
    return (slot_index.reshape(n_rows, per_row), slot_owner)


def mixer_half(queries, key_rows, value_rows, query_gain, key_gain, log_forget, out_weight):
    span_rows = queries.shape[0]
    heads_dev = queries.shape[1] // HEAD_SIZE
    kv_dev = key_rows.shape[1] // HEAD_SIZE
    group_ratio = heads_dev // kv_dev
    scale_qk = HEAD_SIZE ** (-0.5)
    q_normed = head_norm(
        queries.reshape(span_rows, kv_dev, group_ratio, HEAD_SIZE), query_gain
    ).astype(jnp.bfloat16)
    k_normed = head_norm(key_rows.reshape(span_rows, kv_dev, HEAD_SIZE), key_gain).astype(
        jnp.bfloat16
    )
    key_value = jnp.concatenate(
        [k_normed.reshape(span_rows, kv_dev * HEAD_SIZE), value_rows], axis=1
    )
    first_row = lax.axis_index(EP) * span_rows
    last_row = first_row + span_rows - 1
    query_pos = first_row + jnp.arange(span_rows, dtype=jnp.int32)
    query_gates = lax.dynamic_slice_in_dim(log_forget, first_row, span_rows, 1)
    query_gates = query_gates.T.reshape(span_rows, kv_dev, group_ratio)

    def add_block(running, kv_block, key_start):
        run_max, run_sum, run_acc = running
        block_len = kv_block.shape[0]
        k_block = kv_block[:, : kv_dev * HEAD_SIZE].reshape(block_len, kv_dev, HEAD_SIZE)
        v_block = kv_block[:, kv_dev * HEAD_SIZE :].reshape(block_len, kv_dev, HEAD_SIZE)
        key_gates = lax.dynamic_slice_in_dim(log_forget, key_start, block_len, 1)
        key_gates = key_gates.reshape(kv_dev, group_ratio, block_len)
        scores = (
            jnp.einsum("qgrd,kgd->qgrk", q_normed, k_block, preferred_element_type=jnp.float32)
            * scale_qk
        )
        scores = scores + query_gates[..., None] - key_gates[None]
        key_pos = key_start + jnp.arange(block_len, dtype=jnp.int32)
        visible = key_pos[None, :] <= query_pos[:, None]
        scores = jnp.where(visible[:, None, None, :], scores, -jnp.inf)
        new_max = jnp.maximum(run_max, jnp.max(scores, axis=-1))
        shrink = jnp.exp(run_max - new_max)
        weights = jnp.exp(scores - new_max[..., None])
        run_sum = shrink * run_sum + jnp.sum(weights, axis=-1)
        gathered = jnp.einsum(
            "qgrk,kgd->qgrd",
            weights.astype(jnp.bfloat16),
            v_block,
            preferred_element_type=jnp.float32,
        )
        return (new_max, run_sum, shrink[..., None] * run_acc + gathered)

    start_state = (
        jnp.full((span_rows, kv_dev, group_ratio), -jnp.inf, jnp.float32),
        jnp.zeros((span_rows, kv_dev, group_ratio), jnp.float32),
        jnp.zeros((span_rows, kv_dev, group_ratio, HEAD_SIZE), jnp.float32),
    )
    kv_piece = gather_axes(key_value, EP, (0, 1), 0)
    block_len = min(kv_piece.shape[0], span_rows)
    n_blocks = kv_piece.shape[0] // block_len

    def one_block(block_number, running_in):
        key_start = block_number * block_len
        kv_block = lax.dynamic_slice_in_dim(kv_piece, block_number * block_len, block_len, 0)

        def take_block(running_now):
            return add_block(running_now, kv_block, key_start)

        def skip_block(running_now):
            return running_now

        return lax.cond(key_start <= last_row, take_block, skip_block, running_in)

    run_max, run_sum, run_acc = lax.fori_loop(0, n_blocks, one_block, start_state)
    attended = (
        (run_acc / run_sum[..., None])
        .astype(jnp.bfloat16)
        .reshape(span_rows, heads_dev * HEAD_SIZE)
    )
    own_rows = lax.all_to_all(attended, "tp", split_axis=0, concat_axis=1, tiled=True)
    projected = jnp.dot(
        own_rows,
        lax.all_gather(out_weight, "tp", axis=0, tiled=True),
        preferred_element_type=jnp.float32,
    )
    return projected.astype(jnp.bfloat16)


def experts_half(
    expert_rows, expert_gain, routes, route_weight, gate_weight, up_weight, down_weight
):
    n_tp = lax.axis_size("tp")
    n_ep = lax.axis_size(EP)
    span_rows = expert_rows.shape[0]
    model_width = expert_rows.shape[1]
    exp_dev = gate_weight.shape[0]
    capacity = n_tp * ((3 * (span_rows // n_tp) * TOP + 2 * EXPERTS - 1) // (2 * EXPERTS))
    normed = head_norm(expert_rows, expert_gain).astype(jnp.bfloat16)
    slot_index, slot_owner = slot_table(routes.T, EXPERTS, capacity)
    padded = jnp.concatenate([normed, jnp.zeros((1, model_width), jnp.bfloat16)], axis=0)
    part_len = capacity // n_tp
    owner_part = lax.dynamic_slice_in_dim(
        slot_owner.reshape(EXPERTS, capacity), lax.axis_index("tp") * part_len, part_len, 1
    )
    send_rows = padded[owner_part].reshape(n_ep, exp_dev, part_len, model_width)
    arrived = core_and_chips(send_rows, ("ep_0", "ep_1"), (1, 0), 0, 0)
    slot_rows = lax.all_gather(arrived, "tp", axis=2, tiled=True)
    gate_part = jnp.einsum(
        "nxcd,xdf->nxcf", slot_rows, gate_weight, preferred_element_type=jnp.float32
    )
    up_part = jnp.einsum("nxcd,xdf->nxcf", slot_rows, up_weight, preferred_element_type=jnp.float32)
    hidden = (jax.nn.silu(gate_part) * up_part).astype(jnp.bfloat16)
    partial_out = jnp.einsum(
        "nxcf,xfd->nxcd", hidden, down_weight, preferred_element_type=jnp.float32
    )
    summed = lax.psum_scatter(
        partial_out.astype(jnp.bfloat16), "tp", scatter_dimension=3, tiled=True
    )
    returned = lax.all_to_all(summed, EP, split_axis=0, concat_axis=0, tiled=True)
    result_table = returned.reshape(EXPERTS * capacity, returned.shape[3])
    picked = result_table[slot_index]
    combined = jnp.sum(picked.astype(jnp.float32) * route_weight.T[..., None], axis=1)
    return combined.astype(jnp.bfloat16)


def on_device(
    queries,
    key_rows,
    value_rows,
    query_gain,
    key_gain,
    log_forget,
    out_weight,
    expert_rows,
    expert_gain,
    routes,
    route_weight,
    gate_weight,
    up_weight,
    down_weight,
):
    mixer_out = mixer_half(
        queries, key_rows, value_rows, query_gain, key_gain, log_forget, out_weight
    )
    expert_out = experts_half(
        expert_rows, expert_gain, routes, route_weight, gate_weight, up_weight, down_weight
    )
    return (mixer_out, expert_out)


def solution(mesh):
    split = Mesh(
        mesh.devices.reshape(mesh.shape["grp"], 16, 2, mesh.shape["tp"]),
        ("grp", "ep_0", "ep_1", "tp"),
    )
    in_specs = (
        P(GRP_EP, "tp"),
        P(GRP_EP, "tp"),
        P(GRP_EP, "tp"),
        P(),
        P(),
        P("tp", "grp"),
        P("tp", None),
        P(GRP_EP, None),
        P(),
        P(None, GRP_EP),
        P(None, GRP_EP),
        P(EP, None, "tp"),
        P(EP, None, "tp"),
        P(EP, "tp", None),
    )
    out_specs = (P(GRP_EP_TP, None), P(GRP_EP, "tp"))
    return jax.shard_map(
        on_device, mesh=split, in_specs=in_specs, out_specs=out_specs, check_vma=False
    )
```

profile of v0, /device:TPU:46, one launch (start us, length us, event | category | flops | bytes accessed | tf_op | source)
XLA Modules:
  0.0 523.5 jit_solution(8850227480774102825)
XLA Ops:
  9.4 1.6 pad_maximum_fusion
  13.0 15.7 %reduce-window.6 = s32[32,8,128]{2,1,0:T(8,128)S(1)} reduce-window(s32[32,8,128]{2,1,0:T(8,128)} %fusion.46, s32[]{:T(128)} %copy.108), window={size=1x1x128 pad=0_0x0_0x127_0}, to_apply=%region_9.10 | reduce-window | flops 4161536 | bytes 262148 | tf_op jit(solution)/shard_map/reduce-window
  34.7 1.8 compare_select_fusion
  37.6 4.3 scatter_custom_fusion
  43.5 3.1 gather_fusion
  46.6 2.4 reshape_reshape_reshape.3
  49.9 5.0 all_to_all.34
  56.5 105.1 %all_to_all.35 = bf16[16,2,1,1,12,2048]{5,1,4,3,2,0:T(2,128)(2,1)S(1)} all-to-all(bf16[16,2,1,1,12,2048]{5,1,4,3,2,0:T(2,128)(2,1)S(1)} %copy.64), channel_id=1, replica_groups=mesh['grp'=2,'ep_0'=16,'ep_1'=2,'tp'=4] {'ep_0'}, dimensions={0} | all-to-all | bytes 3145728 | tf_op jit(solution)/shard_map/all_to_all | solution.py:45
  163.0 2.0 reshape_reshape.7
  166.1 65.4 %all-gather.10.cloned.1.call-done = bf16[32,1,48,2048]{3,0,1,2:T(8,128)(2,1)} async-done(((bf16[32,1,12,2048]{3,0,1,2:T(8,128)(2,1)}), bf16[32,1,48,2048]{3,0,1,2:T(8,128)(2,1)}) %all-gather.10.cloned.1.call-update) | async-done | bytes 6291472 | tf_op jit(solution)/shard_map/all_gather | solution.py:177
  231.5 8.9 %fusion.14 = f32[32,48,256]{2,1,0:T(8,128)} fusion(bf16[32,1,48,2048]{3,0,1,2:T(8,128)(2,1)} %all-gather.10.cloned.1.call-done, bf16[1,2048,256]{2,1,0:T(8,128)(2,1)S(1)} %copy-done.8), kind=kOutput, calls=%fused_computation.28 | convolution fusion | flops 1610612736 | bytes 8912896 | tf_op jit(solution)/shard_map/nxcd,xdf->nxcf/dot_general | solution.py:178
  240.4 14.0 %convert_bitcast_fusion = bf16[32,1,48,2048]{3,2,0,1:T(8,128)(2,1)} fusion(bf16[1,256,2048]{2,1,0:T(8,128)(2,1)S(1)} %copy-done, bf16[32,1,48,2048]{3,0,1,2:T(8,128)(2,1)} %all-gather.10.cloned.1.call-done, f32[32,48,256]{2,1,0:T(8,128)} %fusion.14, bf16[1,2048,256]{2,1,0:T(8,128)(2,1)S(1)} %copy-done.9), kind=kOutput, calls=%fused_computation.30 | convolution fusion | flops 3226730496 | bytes 16252928 | tf_op jit(solution)/shard_map/nxcf,xfd->nxcd/dot_general | solution.py:183
  256.7 7.3 %all-gather.6.cloned.1.call-done = bf16[32,512,256]{2,1,0:T(8,128)(2,1)} async-done(((bf16[16,512,256]{2,1,0:T(8,128)(2,1)}), bf16[32,512,256]{2,1,0:T(8,128)(2,1)}) %all-gather.6.cloned.1.call-update) | async-done | bytes 8388624 | tf_op jit(solution)/shard_map/all_gather | solution.py:24
  264.0 7.5 %copy.55 = bf16[16,2,512,256]{3,2,1,0:T(8,128)(2,1)} copy(bf16[16,2,512,256]{3,2,0,1:T(8,128)(2,1)} %bitcast.153) | data formatting | bytes 16777216 | tf_op jit(solution)/shard_map/transpose | solution.py:28
  271.6 6.1 %while.18 = (s32[]{:T(128)}, f32[512,1,2]{0,2,1:T(2,128)S(1)}, f32[512,1,2]{0,2,1:T(2,128)S(1)}, f32[512,1,2,128]{0,3,2,1:T(8,128)S(1)}, s32[]{:T(128)}, /*index...) while((s32[]{:T(128)}, f32[512,1,2]{0,2,1:T(2,128)S(1)}, ...), condition=%wide.region_7.8_spmd.clone, body=%wide.region_2.7_spmd.clone.sunk | while | flops 273682432 | bytes 8483165 | solution.py:144
  271.6 4.4 conditional.3
  278.0 12.3 %all_to_all.36 = bf16[4,128,256]{2,1,0:T(8,128)(2,1)S(1)} all-to-all(bf16[4,128,256]{2,1,0:T(8,128)(2,1)S(1)} %copy.73), channel_id=1, replica_groups=mesh['grp'=2,'ep_0'=16,'ep_1'=2,'tp'=4] {'tp'}, dimensions={0} | all-to-all | bytes 524288 | tf_op jit(solution)/shard_map/all_to_all | solution.py:150
  290.3 48.4 %reduce-scatter.2.cloned.1.call-done = bf16[32,1,48,512]{3,2,0,1:T(8,128)(2,1)} async-done(((bf16[32,1,48,2048]{3,2,0,1:T(8,128)(2,1)}), bf16[32,1,48,512]{3,2,0,1:T(8,128)(2,1)}) %reduce-scatter.2.cloned.1.call-update) | async-done | bytes 1572880 | tf_op jit(solution)/shard_map/reduce_scatter | solution.py:186
  338.7 89.1 %all-to-all-start.3 = ((bf16[32,1,48,512]{3,2,1,0:T(8,128)(2,1)}), bf16[32,1,48,512]{3,2,1,0:T(8,128)(2,1)S(1)}, u32[]{:S(2)}, u32[]{:S(2)}) async-start(bf16[32,1,48,512]{3,2,1,0:T(8,128)(2,1)} %bitcast.161), calls=%async_computation.4 | async-start | bytes 3145728 | tf_op jit(solution)/shard_map/all_to_all | solution.py:189
  428.4 3.7 convolution_convert_fusion
  432.2 73.3 %all-to-all-done.3 = bf16[32,1,48,512]{3,2,1,0:T(8,128)(2,1)S(1)} async-done(((bf16[32,1,48,512]{3,2,1,0:T(8,128)(2,1)}), bf16[32,1,48,512]{3,2,1,0:T(8,128)(2,1)S(1)}, u32[]{:S(2)}, u32[]{:S(2)}) %all-to-all-start.3) | async-done | bytes 1572896 | tf_op jit(solution)/shard_map/all_to_all | solution.py:189
  505.4 5.0 gather_fusion.1
  510.5 2.5 reshape.294
  513.0 4.0 multiply_reduce_fusion
  (149 shorter events, 25.6 us)
Async XLA Ops:
  7.2 233.3 %copy-start = (bf16[1,256,2048]{2,1,0:T(8,128)(2,1)S(1)}, bf16[1,256,2048]{2,1,0:T(8,128)(2,1)}, u32[]{:S(2)}) copy-start(bf16[1,256,2048]{2,1,0:T(8,128)(2,1)} %param.31) | copy-start | bytes 3145732
  7.2 157.9 %all-gather.12.cloned.1.call-start = ((), (), s32[]{:S(2)}) async-start(), calls=%async_computation.9 | async-start | bytes 4456448 | tf_op jit(solution)/shard_map/all_gather | solution.py:24
  11.1 31.1 %copy-start.2 = (bf16[512,2048]{1,0:T(8,128)(2,1)S(1)}, bf16[512,2048]{1,0:T(8,128)(2,1)}, u32[]{:S(2)}) copy-start(bf16[512,2048]{1,0:T(8,128)(2,1)} %param.25) | copy-start | bytes 6291460
  11.2 220.3 %all-gather.10.cloned.1.call-start = ((), (), s32[]{:S(2)}) async-start(), calls=%async_computation.7 | async-start | bytes 7864320 | tf_op jit(solution)/shard_map/all_gather | solution.py:177
  32.6 10.0 %copy-start.5 = (f32[2048]{0:T(1024)S(1)}, f32[2048]{0:T(1024)}, u32[]{:S(2)}) copy-start(f32[2048]{0:T(1024)} %param.26) | copy-start | bytes 24580
  165.0 99.0 %all-gather.6.cloned.1.call-start = ((), (), s32[]{:S(2)}) async-start(), calls=%async_computation.5 | async-start | bytes 12582912 | tf_op jit(solution)/shard_map/all_gather | solution.py:24
  165.1 66.4 %copy-start.8 = (bf16[1,2048,256]{2,1,0:T(8,128)(2,1)S(1)}, bf16[1,2048,256]{2,1,0:T(8,128)(2,1)}, u32[]{:S(2)}) copy-start(bf16[1,2048,256]{2,1,0:T(8,128)(2,1)} %param.29) | copy-start | bytes 3145732
  165.8 74.6 %copy-start.9 = (bf16[1,2048,256]{2,1,0:T(8,128)(2,1)S(1)}, bf16[1,2048,256]{2,1,0:T(8,128)(2,1)}, u32[]{:S(2)}) copy-start(bf16[1,2048,256]{2,1,0:T(8,128)(2,1)} %param.30) | copy-start | bytes 3145732
  165.8 172.9 %reduce-scatter.2.cloned.1.call-start = ((), (), s32[]{:S(2)}) async-start(), calls=%async_computation.8 | async-start | bytes 7864320 | tf_op jit(solution)/shard_map/reduce_scatter | solution.py:186
  254.4 1.0 copy-start.4
  254.4 1.2 copy-start.7
  254.5 173.9 %all-gather.8.cloned.1.call-start = ((), (), s32[]{:S(2)}) async-start(), calls=%async_computation.6 | async-start | bytes 5242880 | tf_op jit(solution)/shard_map/all_gather | solution.py:153
  277.8 150.0 %copy-start.3 = (s32[512,2]{1,0:T(8,128)S(1)}, s32[512,2]{1,0:T(8,128)}, u32[]{:S(2)}) copy-start(s32[512,2]{1,0:T(8,128)} %get-tuple-element.369) | copy-start | bytes 12292
  278.0 150.0 %copy-start.6 = (f32[2,512]{1,0:T(2,128)S(1)}, f32[2,512]{1,0:T(2,128)}, u32[]{:S(2)}) copy-start(f32[2,512]{1,0:T(2,128)} %param.28) | copy-start | bytes 12292
  338.7 166.7 %all-to-all-start.3 = ((bf16[32,1,48,512]{3,2,1,0:T(8,128)(2,1)}), bf16[32,1,48,512]{3,2,1,0:T(8,128)(2,1)S(1)}, u32[]{:S(2)}, u32[]{:S(2)}) async-start(bf16[32,1,48,512]{3,2,1,0:T(8,128)(2,1)} %bitcast.161), calls=%async_computation.4 | async-start | bytes 3145728 | tf_op jit(solution)/shard_map/all_to_all | solution.py:189
  510.5 6.5 %copy-start.1 = (bf16[1,256,2048]{2,1,0:T(8,128)(2,1)S(1)}, bf16[1,256,2048]{2,1,0:T(8,128)(2,1)}, u32[]{:S(2)}) copy-start(bf16[1,256,2048]{2,1,0:T(8,128)(2,1)} %param.31) | copy-start | bytes 3145732
Sparse Core Ops, SparseCore 0:
  11.3 142.5 all-gather.11
  165.1 66.3 all-gather.9
  233.3 30.6 all-gather.5
  266.4 72.2 reduce-scatter.1
  340.4 51.5 all-gather.7
where the time goes:
time: 531 us; the launch traced here: 524 us
  waiting for transfers between devices  196 us (37%)
  blocking collectives  122 us (23%)
  starting transfers between devices  89.6 us (17%)
  local copies, waits for them, and re-layouts  40.4 us (8%)
  matrix products  29.7 us (6%)
  other arithmetic  29.6 us (6%)
  between operations  14.1 us (3%)
    all_to_all x2, blocking collectives, turned_blocks(): lax.all_to_all(parts, axes[k], split_axis=k, concat_axis=k, tiled=True)  110 us
    all_to_all x1, starting transfers between devices, experts_half(): lax.all_to_all(summed, EP, split_axis=0, concat_axis=0, tiled=True)  89.1 us
    all_to_all x1, waiting for transfers between devices, experts_half(): lax.all_to_all(summed, EP, split_axis=0, concat_axis=0, tiled=True)  73.3 us
    all_gather x1, waiting for transfers between devices, experts_half(): slot_rows = lax.all_gather(arrived, 'tp', axis=2, tiled=True)  65.4 us
    reduce_scatter x1, waiting for transfers between devices, experts_half(): lax.psum_scatter(partial_out.astype(jnp.bfloat16), 'tp', scatter_dimensio...  48.4 us
    another operation x2, other arithmetic  15.7 us
    dot_general x1, matrix products, experts_half(): jnp.einsum('nxcf,xfd->nxcd', hidden, down_weight, preferred_element_type=...  14 us
    all_to_all x1, blocking collectives, mixer_half(): lax.all_to_all(attended, 'tp', split_axis=0, concat_axis=1, tiled=True)  12.3 us
  transfers between devices with their start and end apart: 6, of which 4 were waited for; matrix products, arithmetic and copies ran while one was open for 16% of the time, Pallas kernels for 0%

commit v1 on v0

v1 whole, which is shorter than its diff:
```python
import functools

import jax
import jax.numpy as jnp
from jax import lax
from jax.experimental import pallas as pl
from jax.experimental.pallas import tpu as pltpu
from jax.sharding import PartitionSpec as P

HEAD_SIZE = 128
EXPERTS = 32
CAP = 48
TOP = 2
CORES = 2
LOG2E = 1.4426950408889634
MESH = pl.DeviceIdType.MESH
F32 = jnp.float32
BF16 = jnp.bfloat16


def dot(a, b, dims=(((1,), (0,)), ((), ()))):
    return lax.dot_general(a, b, dims, preferred_element_type=F32)


def row_norm(rows, gain):
    wide = rows.astype(F32)
    factor = lax.rsqrt(jnp.mean(wide * wide, axis=-1, keepdims=True) + 1e-06)
    return wide * factor * gain


def member_and_rank(routes, expert_col):
    tokens = routes.shape[1]
    count = expert_col.shape[0]
    named = jnp.logical_or(routes[0:1, :] == expert_col, routes[1:2, :] == expert_col)
    member = jnp.where(named, 1.0, 0.0).astype(F32)
    before = lax.broadcasted_iota(jnp.int32, (tokens, tokens), 0)
    after = lax.broadcasted_iota(jnp.int32, (tokens, tokens), 1)
    earlier = jnp.where(before < after, 1.0, 0.0).astype(BF16)
    del count
    return member, dot(member.astype(BF16), earlier)


def prologue_kernel(
    n_tp, rows_ref, gain_ref, routes_ref, key_ref, value_ref, key_gain_ref, send_ref, kv_ref, normed
):
    span = rows_ref.shape[0]
    me, t = lax.axis_index("ep"), lax.axis_index("tp")
    offset = lax.rem(t + (n_tp - 1) * me, n_tp)
    kv_ref[:, :HEAD_SIZE] = row_norm(key_ref[...], key_gain_ref[...]).astype(BF16)
    kv_ref[:, HEAD_SIZE:] = value_ref[...]
    step = 64
    for first in range(0, span, step):
        normed[first : first + step, :] = row_norm(
            rows_ref[first : first + step, :], gain_ref[...]
        ).astype(BF16)
    here = EXPERTS // n_tp
    expert_col = offset + n_tp * lax.broadcasted_iota(jnp.int32, (here, 1), 0)
    member, rank = member_and_rank(routes_ref[...], expert_col)
    place = jnp.where(member > 0.5, rank, -1.0)
    slot = lax.broadcasted_iota(jnp.int32, (CAP, span), 0).astype(F32)
    for m in range(here):
        pick = jnp.where(place[m : m + 1, :] == slot, 1.0, 0.0).astype(BF16)
        send_ref[m] = dot(pick, normed[...]).astype(BF16)


def spread_kernel(
    n_ep,
    n_tp,
    send_ref,
    kv_ref,
    gate_ref,
    up_ref,
    down_ref,
    out_ref,
    recv_ref,
    kv_all,
    gate_all,
    up_all,
    down_all,
    out_all,
    row_send,
    row_recv,
    fwd_send,
    fwd_recv,
    bwd_send,
    bwd_recv,
    core_send,
    core_recv,
    side_send,
    side_recv,
    half_send,
    half_recv,
    local,
):
    me, t = lax.axis_index("ep"), lax.axis_index("tp")
    n_z = n_ep // CORES
    z, core = me // CORES, lax.rem(me, CORES)
    offset = lax.rem(t + (n_tp - 1) * me, n_tp)
    here = n_ep // n_tp
    right, left = lax.rem(t + 1, n_tp), lax.rem(t + n_tp - 1, n_tp)
    across = lax.rem(t + 2, n_tp)
    up_ep = CORES * lax.rem(z + 1, n_z) + core
    down_ep = CORES * lax.rem(z + n_z - 1, n_z) + core
    other = CORES * z + (1 - core)
    reach = n_z // 2
    self_slot = me // n_tp
    is_self = lax.rem(me, n_tp) == offset

    barrier = pltpu.get_barrier_semaphore()
    for where in (
        {"ep": up_ep},
        {"ep": down_ep},
        {"ep": other},
        {"tp": right},
        {"tp": left},
    ):
        pl.semaphore_signal(barrier, inc=1, device_id=where, device_id_type=MESH)
    for m in range(here):
        mate = offset + n_tp * m

        @pl.when(mate != me)
        def _():
            pl.semaphore_signal(barrier, inc=1, device_id={"ep": mate}, device_id_type=MESH)

    pl.semaphore_wait(barrier, 5 + here - jnp.where(is_self, 1, 0))

    def remote(src, dst, send_sem, recv_sem, where):
        return pltpu.make_async_remote_copy(
            src_ref=src,
            dst_ref=dst,
            send_sem=send_sem,
            recv_sem=recv_sem,
            device_id=where,
            device_id_type=MESH,
        )

    arrays = ((gate_ref, gate_all), (up_ref, up_all), (down_ref, down_all))
    out_rows = out_ref.shape[0] // CORES
    out_first = core * out_rows

    def side_copy(a, to_right):
        where = {"tp": right} if to_right else {"tp": left}
        way = 0 if to_right else 1
        if a < 3:
            src, dst = arrays[a][0], arrays[a][1].at[t]
        else:
            mine = pl.ds(out_first, out_rows)
            src, dst = out_ref.at[mine], out_all.at[t, mine]
        return remote(src, dst, side_send.at[a, way], side_recv.at[a, way], where)

    def half_copy(a, to_right):
        where = {"tp": right} if to_right else {"tp": left}
        way = 0 if to_right else 1
        owner = left if to_right else right
        if a < 3:
            full = arrays[a][1]
            half = full.shape[1] // 2
            part = full.at[owner, pl.ds(way * half, half)]
        else:
            half = out_rows // 2
            part = out_all.at[owner, pl.ds(out_first + way * half, half)]
        return remote(part, part, half_send.at[a, way], half_recv.at[a, way], where)

    def out_copy(k):
        owner = (left, right, across)[k]
        part = out_all.at[owner, pl.ds(out_first, out_rows)]
        return remote(part, part, core_send.at[k], core_recv.at[k], {"ep": other})

    def kv_copy(source_z, source_core, send_sem, recv_sem, where, own=False):
        block = kv_all.at[CORES * source_z + source_core]
        return remote(kv_ref if own else block, block, send_sem, recv_sem, where)

    def fwd_copy(s):
        return kv_copy(
            lax.rem(z - s + n_z, n_z), core, fwd_send.at[s], fwd_recv.at[s], {"ep": up_ep}, s == 0
        )

    def bwd_copy(s):
        return kv_copy(
            lax.rem(z + s, n_z), core, bwd_send.at[s], bwd_recv.at[s], {"ep": down_ep}, s == 0
        )

    def row_copy(k):
        m = lax.rem(self_slot + k, here)
        mate = offset + n_tp * m
        return mate, remote(
            send_ref.at[m],
            recv_ref.at[self_slot],
            row_send.at[m],
            row_recv.at[self_slot],
            {"ep": mate},
        )

    def row_local():
        return pltpu.make_async_copy(
            send_ref.at[self_slot], recv_ref.at[self_slot], local.at[5]
        )

    def fwd_sends(s):
        return jnp.logical_and(z - s >= 0, z + 1 <= n_z - 1)

    def fwd_gets(s):
        return z - 1 - s >= 0

    def bwd_sends(s):
        return lax.rem(z + s, n_z) <= reach - 2

    def bwd_gets(s):
        return lax.rem(z + 1 + s, n_z) <= reach - 2

    def bwd_needed(s):
        return jnp.logical_and(bwd_gets(s), lax.rem(z + 1 + s, n_z) < z)

    for a in range(4):
        side_copy(a, True).start()
        side_copy(a, False).start()
    own = [
        pltpu.make_async_copy(kv_ref, kv_all.at[me], local.at[0]),
        pltpu.make_async_copy(gate_ref, gate_all.at[t], local.at[1]),
        pltpu.make_async_copy(up_ref, up_all.at[t], local.at[2]),
        pltpu.make_async_copy(down_ref, down_all.at[t], local.at[3]),
        pltpu.make_async_copy(out_ref, out_all.at[t], local.at[4]),
    ]
    for copy in own:
        copy.start()

    @pl.when(is_self)
    def _():
        row_local().start()

    def core_own():
        return kv_copy(z, core, core_send.at[3], core_recv.at[3], {"ep": other}, True)

    def core_fwd(s, source_core):
        return kv_copy(
            lax.rem(z - 1 - s + n_z, n_z),
            source_core,
            core_send.at[4 + s],
            core_recv.at[4 + s],
            {"ep": other},
        )

    def core_bwd(s, source_core):
        return kv_copy(
            lax.rem(z + 1 + s, n_z),
            source_core,
            core_send.at[4 + reach + s],
            core_recv.at[4 + reach + s],
            {"ep": other},
        )

    @pl.when(core == 0)
    def _():
        core_own().start()

    for s in range(reach):
        if s > 0:

            @pl.when(fwd_gets(s - 1))
            def _():
                fwd_copy_in(kv_copy, kv_all, z, n_z, core, s - 1, fwd_send, fwd_recv, up_ep)
                core_fwd(s - 1, core).start()

        @pl.when(fwd_sends(s))
        def _():
            fwd_copy(s).start()

        if s < reach - 1:
            if s > 0:

                @pl.when(bwd_gets(s - 1))
                def _():
                    bwd_copy_in(kv_copy, z, n_z, core, s - 1, bwd_send, bwd_recv, down_ep)

                @pl.when(bwd_needed(s - 1))
                def _():
                    core_bwd(s - 1, core).start()

            @pl.when(bwd_sends(s))
            def _():
                bwd_copy(s).start()

        mate, copy = row_copy(s)

        @pl.when(mate != me)
        def _(copy=copy):
            copy.start()

        if s in (2, 4, 6):
            a = (2, 4, 6).index(s)
            side_copy(a, True).wait_recv()
            half_copy(a, True).start()
            side_copy(a, False).wait_recv()
            half_copy(a, False).start()

    last = reach - 1

    @pl.when(fwd_gets(last))
    def _():
        fwd_copy_in(kv_copy, kv_all, z, n_z, core, last, fwd_send, fwd_recv, up_ep)
        core_fwd(last, core).start()

    @pl.when(bwd_gets(last - 1))
    def _():
        bwd_copy_in(kv_copy, z, n_z, core, last - 1, bwd_send, bwd_recv, down_ep)

    @pl.when(bwd_needed(last - 1))
    def _():
        core_bwd(last - 1, core).start()

    side_copy(3, True).wait_recv()
    half_copy(3, True).start()
    side_copy(3, False).wait_recv()
    half_copy(3, False).start()
    out_copy(0).start()
    out_copy(1).start()
    half_copy(3, True).wait_recv()
    half_copy(3, False).wait_recv()
    out_copy(2).start()

    for a in range(4):
        for to_right in (True, False):
            side_copy(a, to_right).wait_send()
            if a < 3:
                half_copy(a, to_right).wait_recv()
            half_copy(a, to_right).wait_send()
    for k in range(here):
        mate, copy = row_copy(k)

        @pl.when(mate != me)
        def _(copy=copy):
            copy.wait_send()

        source = offset + n_tp * k
        arrival = remote(
            send_ref.at[k], recv_ref.at[k], row_send.at[k], row_recv.at[k], {"ep": source}
        )

        @pl.when(source != me)
        def _(arrival=arrival):
            arrival.wait_recv()

    for s in range(reach):

        @pl.when(fwd_sends(s))
        def _():
            fwd_copy(s).wait_send()

        @pl.when(fwd_gets(s))
        def _():
            core_fwd(s, core).wait_send()
            core_fwd(s, 1 - core).wait_recv()

        if s < reach - 1:

            @pl.when(bwd_sends(s))
            def _():
                bwd_copy(s).wait_send()

            @pl.when(bwd_needed(s))
            def _():
                core_bwd(s, core).wait_send()
                core_bwd(s, 1 - core).wait_recv()

    for k in range(3):
        out_copy(k).wait_send()
        out_first_other = (1 - core) * out_rows
        owner = (left, right, across)[k]
        part = out_all.at[owner, pl.ds(out_first_other, out_rows)]
        remote(part, part, core_send.at[k], core_recv.at[k], {"ep": other}).wait_recv()

    @pl.when(core == 0)
    def _():
        core_own().wait_send()

    @pl.when(core == 1)
    def _():
        kv_copy(z, 0, core_send.at[3], core_recv.at[3], {"ep": other}).wait_recv()

    for copy in own:
        copy.wait()

    @pl.when(is_self)
    def _():
        row_local().wait()


def fwd_copy_in(kv_copy, kv_all, z, n_z, core, s, send, recv, up_ep):
    kv_copy(
        lax.rem(z - 1 - s + n_z, n_z), core, send.at[s], recv.at[s], {"ep": up_ep}
    ).wait_recv()


def bwd_copy_in(kv_copy, z, n_z, core, s, send, recv, down_ep):
    kv_copy(lax.rem(z + 1 + s, n_z), core, send.at[s], recv.at[s], {"ep": down_ep}).wait_recv()


def split_three(value):
    high = value.astype(BF16)
    rest = value - high.astype(F32)
    mid = rest.astype(BF16)
    low = (rest - mid.astype(F32)).astype(BF16)
    return high.astype(F32), mid.astype(F32), low.astype(F32)


def attention_kernel(
    heads,
    query_ref,
    gain_ref,
    forget_ref,
    kv_ref,
    out_ref,
    query_t,
    run_max,
    run_sum,
    acc,
):
    span = query_ref.shape[0]
    me = lax.axis_index("ep")
    scale = HEAD_SIZE ** (-0.5)
    exp_scale = scale * LOG2E
    columns = heads * span
    for h in range(heads):
        normed = row_norm(query_ref[:, h * HEAD_SIZE : (h + 1) * HEAD_SIZE], gain_ref[...])
        rounded = normed.astype(BF16).astype(F32)
        query_t[:HEAD_SIZE, h * span : (h + 1) * span] = rounded.T.astype(BF16)
    row = lax.broadcasted_iota(jnp.int32, (HEAD_SIZE, columns), 0)
    head = lax.broadcasted_iota(jnp.int32, (HEAD_SIZE, columns), 1) // span
    query_t[HEAD_SIZE:, :] = jnp.where(row // 3 == head, 1.0, 0.0).astype(BF16)
    run_max[...] = jnp.full(run_max.shape, -1e30, F32)
    run_sum[...] = jnp.zeros(run_sum.shape, F32)
    acc[...] = jnp.zeros(acc.shape, F32)
    lane = lax.broadcasted_iota(jnp.int32, (8, HEAD_SIZE), 1)
    sub = lax.broadcasted_iota(jnp.int32, (8, HEAD_SIZE), 0)
    place = jnp.where(lane == sub, 1.0, 0.0).astype(BF16)
    width = 256

    def add_block(block, masked):
        first = pl.multiple_of(block * span, span)
        rows = []
        for h in range(heads):
            gates = forget_ref[h : h + 1, pl.ds(first, span)]
            rows.extend(split_three(gates * (-1.0 / scale)))
        rows.append(jnp.zeros((8 - len(rows), span), F32))
        stacked = jnp.concatenate(rows, axis=0).astype(BF16)
        bias = dot(stacked, place, (((0,), (0,)), ((), ()))).astype(BF16)
        keys = jnp.concatenate([kv_ref[block, :, :HEAD_SIZE], bias], axis=1)
        values = kv_ref[block, :, HEAD_SIZE:]
        for first_col in range(0, columns, width):
            cols = slice(first_col, first_col + width)
            scores = dot(keys, query_t[:, cols])
            if masked:
                key_at = lax.broadcasted_iota(jnp.int32, (span, width), 0)
                query_at = lax.broadcasted_iota(jnp.int32, (span, width), 1) + first_col % span
                scores = jnp.where(key_at <= query_at, scores, -1e30)
            old_max = run_max[:, cols]
            new_max = jnp.maximum(old_max, jnp.max(scores, axis=0, keepdims=True))
            shrink = jnp.exp2((old_max - new_max) * exp_scale)
            weights = jnp.exp2((scores - new_max) * exp_scale)
            run_max[:, cols] = new_max
            run_sum[:, cols] = shrink * run_sum[:, cols] + jnp.sum(weights, axis=0, keepdims=True)
            gathered = dot(values, weights.astype(BF16), (((0,), (0,)), ((), ())))
            acc[:, cols] = shrink * acc[:, cols] + gathered

    def body(block, carry):
        add_block(block, False)
        return carry

    lax.fori_loop(0, me, body, 0)
    add_block(me, True)
    for h in range(heads):
        cols = slice(h * span, (h + 1) * span)
        attended = (acc[:, cols] / run_sum[:, cols]).T
        out_ref[:, h * HEAD_SIZE : (h + 1) * HEAD_SIZE] = attended.astype(BF16)


def expert_kernel(rows_ref, gate_ref, up_ref, down_ref, out_ref, total):
    p = pl.program_id(0)
    parts, sources = out_ref.shape[0], out_ref.shape[1]
    width = out_ref.shape[3]
    rows = rows_ref[...]
    gate = dot(rows, gate_ref[0])
    up = dot(rows, up_ref[0])
    hidden = (gate / (1.0 + jnp.exp(-gate)) * up).astype(BF16)

    @pl.when(p == 0)
    def _():
        total[...] = jnp.zeros(total.shape, F32)

    for q in range(parts):
        cols = slice(q * width, (q + 1) * width)
        piece = dot(hidden, down_ref[0, :, cols]).astype(BF16).astype(F32)
        total[:, cols] += piece

    @pl.when(p == pl.num_programs(0) - 1)
    def _():
        for q in range(parts):
            for n in range(sources):
                out_ref[q, n] = total[
                    n * CAP : (n + 1) * CAP, q * width : (q + 1) * width
                ].astype(BF16)


def return_kernel(
    n_ep,
    n_tp,
    result_ref,
    attended_ref,
    back_ref,
    heads_ref,
    row_send,
    row_recv,
    head_send,
    head_recv,
    local,
):
    me, t = lax.axis_index("ep"), lax.axis_index("tp")
    offset = lax.rem(t + (n_tp - 1) * me, n_tp)
    here = n_ep // n_tp
    token_rows = attended_ref.shape[0] // n_tp
    self_slot = me // n_tp
    is_self = lax.rem(me, n_tp) == offset

    barrier = pltpu.get_barrier_semaphore()
    for e in range(n_ep):
        column = lax.rem(me + e, n_tp)

        @pl.when(jnp.logical_not(jnp.logical_and(me == e, column == t)))
        def _(e=e, column=column):
            pl.semaphore_signal(
                barrier, inc=1, device_id={"ep": e, "tp": column}, device_id_type=MESH
            )

    for k in range(1, n_tp):
        pl.semaphore_signal(
            barrier, inc=1, device_id={"tp": lax.rem(t + k, n_tp)}, device_id_type=MESH
        )
    pl.semaphore_wait(barrier, n_ep + n_tp - 1 - jnp.where(is_self, 1, 0))

    def remote(src, dst, send_sem, recv_sem, where):
        return pltpu.make_async_remote_copy(
            src_ref=src,
            dst_ref=dst,
            send_sem=send_sem,
            recv_sem=recv_sem,
            device_id=where,
            device_id_type=MESH,
        )

    def head_copy(k):
        q = lax.rem(t + k, n_tp)
        first = pl.multiple_of(q * token_rows, token_rows)
        return remote(
            attended_ref.at[pl.ds(first, token_rows)],
            heads_ref.at[t],
            head_send.at[k],
            head_recv.at[k],
            {"tp": q},
        )

    own_first = pl.multiple_of(t * token_rows, token_rows)
    own_heads = pltpu.make_async_copy(
        attended_ref.at[pl.ds(own_first, token_rows)], heads_ref.at[t], local.at[0]
    )
    own_row = pltpu.make_async_copy(result_ref.at[t, self_slot], back_ref.at[me], local.at[1])

    def row_copy(k, j):
        n = lax.rem(self_slot + k, here)
        q = lax.rem(t + j, n_tp)
        target = offset + n_tp * n
        away = jnp.logical_not(jnp.logical_and(target == me, q == t))
        return away, remote(
            result_ref.at[q, n],
            back_ref.at[me],
            row_send.at[k, j],
            row_recv.at[me],
            {"ep": target, "tp": q},
        )

    for k in range(1, n_tp):
        head_copy(k).start()
    own_heads.start()

    @pl.when(is_self)
    def _():
        own_row.start()

    for k in range(here):
        for j in range(n_tp):
            away, copy = row_copy(k, j)

            @pl.when(away)
            def _(copy=copy):
                copy.start()

    for k in range(here):
        for j in range(n_tp):
            away, copy = row_copy(k, j)

            @pl.when(away)
            def _(copy=copy):
                copy.wait_send()

    for e in range(n_ep):
        column = lax.rem(me + e, n_tp)
        arrival = remote(
            result_ref.at[0, 0],
            back_ref.at[e],
            row_send.at[0, 0],
            row_recv.at[e],
            {"ep": e, "tp": column},
        )

        @pl.when(jnp.logical_not(jnp.logical_and(me == e, column == t)))
        def _(arrival=arrival):
            arrival.wait_recv()

    for k in range(1, n_tp):
        source = lax.rem(t + n_tp - k, n_tp)
        head_copy(k).wait_send()
        remote(
            attended_ref.at[pl.ds(0, token_rows)],
            heads_ref.at[source],
            head_send.at[k],
            head_recv.at[k],
            {"tp": source},
        ).wait_recv()
    own_heads.wait()

    @pl.when(is_self)
    def _():
        own_row.wait()


def combine_kernel(back_ref, routes_ref, weight_ref, heads_ref, out_w_ref, mixer_ref, out_ref):
    slots = back_ref.shape[0]
    span = routes_ref.shape[1]
    expert_col = lax.broadcasted_iota(jnp.int32, (EXPERTS, 1), 0)
    routes = routes_ref[...]
    _, rank = member_and_rank(routes, expert_col)
    total = None
    for j in range(TOP):
        chosen = routes[j : j + 1, :]
        within = jnp.sum(jnp.where(chosen == expert_col, rank, 0.0), axis=0, keepdims=True)
        slot = chosen * CAP + within.astype(jnp.int32)
        at = lax.broadcasted_iota(jnp.int32, (slots, span), 0)
        pick = jnp.where(at == slot, 1.0, 0.0).astype(BF16)
        picked = dot(pick, back_ref[...], (((0,), (0,)), ((), ())))
        term = picked * weight_ref[:, j : j + 1]
        total = term if total is None else total + term
    out_ref[...] = total.astype(BF16)
    projected = None
    for k in range(heads_ref.shape[0]):
        piece = dot(heads_ref[k], out_w_ref[k])
        projected = piece if projected is None else projected + piece
    mixer_ref[...] = projected.astype(BF16)


def on_device(
    n_ep,
    n_tp,
    queries,
    key_rows,
    value_rows,
    query_gain,
    key_gain,
    log_forget,
    out_weight,
    expert_rows,
    expert_gain,
    routes,
    route_weight,
    gate_weight,
    up_weight,
    down_weight,
):
    span, model_width = expert_rows.shape
    here = n_ep // n_tp
    heads = queries.shape[1] // HEAD_SIZE
    width = model_width // n_tp
    n_z = n_ep // CORES
    reach = n_z // 2
    ff_part = gate_weight.shape[2]
    hbm = pl.BlockSpec(memory_space=pltpu.HBM)
    vmem = pl.BlockSpec(memory_space=pltpu.VMEM)
    shape = jax.ShapeDtypeStruct
    big = pltpu.CompilerParams(vmem_limit_bytes=56 * 1024 * 1024)

    send_rows, key_value = pl.pallas_call(
        functools.partial(prologue_kernel, n_tp),
        out_shape=(
            shape((here, CAP, model_width), BF16),
            shape((span, 2 * HEAD_SIZE), BF16),
        ),
        in_specs=[vmem] * 6,
        out_specs=(vmem, vmem),
        scratch_shapes=[pltpu.VMEM((span, model_width), BF16)],
        compiler_params=big,
        name="prologue",
    )(
        expert_rows,
        expert_gain.reshape(1, -1),
        routes,
        key_rows,
        value_rows,
        key_gain.reshape(1, -1),
    )

    dma = pltpu.SemaphoreType.DMA
    recv_rows, kv_all, gate_all, up_all, down_all, out_all = pl.pallas_call(
        functools.partial(spread_kernel, n_ep, n_tp),
        out_shape=(
            shape((here, CAP, model_width), BF16),
            shape((n_ep, span, 2 * HEAD_SIZE), BF16),
            shape((n_tp, model_width, ff_part), BF16),
            shape((n_tp, model_width, ff_part), BF16),
            shape((n_tp, ff_part, model_width), BF16),
            shape((n_tp, *out_weight.shape), BF16),
        ),
        in_specs=[hbm] * 6,
        out_specs=(hbm,) * 6,
        scratch_shapes=[
            dma((here,)),
            dma((here,)),
            dma((reach,)),
            dma((reach,)),
            dma((reach - 1,)),
            dma((reach - 1,)),
            dma((4 + 2 * reach,)),
            dma((4 + 2 * reach,)),
            dma((4, 2)),
            dma((4, 2)),
            dma((4, 2)),
            dma((4, 2)),
            dma((6,)),
        ],
        compiler_params=pltpu.CompilerParams(collective_id=0, has_side_effects=True),
        name="spread",
    )(
        send_rows,
        key_value,
        gate_weight.reshape(model_width, ff_part),
        up_weight.reshape(model_width, ff_part),
        down_weight.reshape(ff_part, model_width),
        out_weight,
    )

    results = pl.pallas_call(
        expert_kernel,
        grid=(n_tp,),
        out_shape=shape((n_tp, here, CAP, width), BF16),
        in_specs=[
            pl.BlockSpec((here * CAP, model_width), lambda p: (0, 0)),
            pl.BlockSpec((1, model_width, ff_part), lambda p: (p, 0, 0)),
            pl.BlockSpec((1, model_width, ff_part), lambda p: (p, 0, 0)),
            pl.BlockSpec((1, ff_part, model_width), lambda p: (p, 0, 0)),
        ],
        out_specs=pl.BlockSpec((n_tp, here, CAP, width), lambda p: (0, 0, 0, 0)),
        scratch_shapes=[pltpu.VMEM((here * CAP, model_width), F32)],
        compiler_params=pltpu.CompilerParams(
            dimension_semantics=("arbitrary",), vmem_limit_bytes=56 * 1024 * 1024
        ),
        name="experts",
    )(recv_rows.reshape(here * CAP, model_width), gate_all, up_all, down_all)

    columns = heads * span
    attended = pl.pallas_call(
        functools.partial(attention_kernel, heads),
        out_shape=shape((span, heads * HEAD_SIZE), BF16),
        in_specs=[vmem] * 4,
        out_specs=vmem,
        scratch_shapes=[
            pltpu.VMEM((2 * HEAD_SIZE, columns), BF16),
            pltpu.VMEM((1, columns), F32),
            pltpu.VMEM((1, columns), F32),
            pltpu.VMEM((HEAD_SIZE, columns), F32),
        ],
        compiler_params=big,
        name="attention",
    )(queries, query_gain.reshape(1, -1), log_forget, kv_all)

    back_rows, head_rows = pl.pallas_call(
        functools.partial(return_kernel, n_ep, n_tp),
        out_shape=(
            shape((n_ep, CAP, width), BF16),
            shape((n_tp, span // n_tp, heads * HEAD_SIZE), BF16),
        ),
        in_specs=[hbm] * 2,
        out_specs=(hbm, hbm),
        scratch_shapes=[
            dma((here, n_tp)),
            dma((n_ep,)),
            dma((n_tp,)),
            dma((n_tp,)),
            dma((2,)),
        ],
        compiler_params=pltpu.CompilerParams(collective_id=1, has_side_effects=True),
        name="give_back",
    )(results, attended)

    mixer_out, expert_out = pl.pallas_call(
        combine_kernel,
        out_shape=(
            shape((span // n_tp, model_width), BF16),
            shape((span, width), BF16),
        ),
        in_specs=[vmem] * 5,
        out_specs=(vmem, vmem),
        compiler_params=big,
        name="combine",
    )(back_rows.reshape(n_ep * CAP, width), routes, route_weight.T, head_rows, out_all)
    return (mixer_out, expert_out)


def solution(mesh):
    in_specs = (
        P(("grp", "ep"), "tp"),
        P(("grp", "ep"), "tp"),
        P(("grp", "ep"), "tp"),
        P(),
        P(),
        P("tp", "grp"),
        P("tp", None),
        P(("grp", "ep"), None),
        P(),
        P(None, ("grp", "ep")),
        P(None, ("grp", "ep")),
        P("ep", None, "tp"),
        P("ep", None, "tp"),
        P("ep", "tp", None),
    )
    out_specs = (P(("grp", "ep", "tp"), None), P(("grp", "ep"), "tp"))
    return jax.shard_map(
        functools.partial(on_device, mesh.shape["ep"], mesh.shape["tp"]),
        mesh=mesh,
        in_specs=in_specs,
        out_specs=out_specs,
        check_vma=False,
    )
```

time: 531 us -> 364 us (0.69); the launches traced: 524 us -> 364 us
  Pallas kernels: 0 us -> 362 us
  waiting for transfers between devices: 196 us -> 0 us
  blocking collectives: 122 us -> 0 us
  starting transfers between devices: 89.6 us -> 0 us
  local copies, waits for them, and re-layouts: 40.4 us -> 0.87 us
  matrix products: 29.7 us -> 0 us
  other arithmetic: 29.6 us -> 0 us
  between operations: 14.1 us -> 0.66 us
    pallas_call x0 -> x6, Pallas kernels: none -> 362 us  [the longest x1 197 us: on_device(): pl.pallas_call(functools.partial(spread_kernel, n_ep, n_tp), out_shape=(s...]
    all_to_all x3 -> x0, blocking collectives: 122 us -> none  [the longest x2 110 us: turned_blocks(): lax.all_to_all(parts, axes[k], split_axis=k, concat_axis=k, tiled=True)]
    all_to_all x1 -> x0, starting transfers between devices: 89.1 us -> none  [experts_half(): lax.all_to_all(summed, EP, split_axis=0, concat_axis=0, tiled=True)]
    all_to_all x1 -> x0, waiting for transfers between devices: 73.3 us -> none  [experts_half(): lax.all_to_all(summed, EP, split_axis=0, concat_axis=0, tiled=True)]
    all_gather x4 -> x0, waiting for transfers between devices: 72.8 us -> none  [the longest x1 65.4 us: experts_half(): slot_rows = lax.all_gather(arrived, 'tp', axis=2, tiled=True)]
    reduce_scatter x1 -> x0, waiting for transfers between devices: 48.4 us -> none  [experts_half(): lax.psum_scatter(partial_out.astype(jnp.bfloat16), 'tp', scatter_dimensio...]
    dot_general x5 -> x0, matrix products: 29.7 us -> none  [the longest x1 14 us: experts_half(): jnp.einsum('nxcf,xfd->nxcd', hidden, down_weight, preferred_element_type=...]
    another operation x2 -> x0, other arithmetic: 15.7 us -> none
  transfers between devices with their start and end apart: 6 -> 0, of which waited for: 4 -> 0; matrix products, arithmetic and copies ran while one was open for 16% -> 0% of each run, Pallas kernels for 0% -> 0%
where the time goes in v1:
time: 364 us
  Pallas kernels  362 us (99%)
    pallas_call x1, Pallas kernels, on_device(): pl.pallas_call(functools.partial(spread_kernel, n_ep, n_tp), out_shape=(s...  197 us
    pallas_call x1, Pallas kernels, on_device(): pl.pallas_call(functools.partial(return_kernel, n_ep, n_tp), out_shape=(s...  135 us
    pallas_call x1, Pallas kernels, on_device(): pl.pallas_call(expert_kernel, grid=(n_tp,), out_shape=shape((n_tp, here,...  10.9 us

profile of v1, /device:TPU:46, one launch (start us, length us, event | category | flops | bytes accessed | tf_op | source)
XLA Modules:
  0.0 363.7 jit_solution(6150767705952087105)
XLA Ops:
  0.6 6.6 %prologue.1 = (bf16[8,48,2048]{2,1,0:T(8,128)(2,1)}, bf16[512,256]{1,0:T(8,128)(2,1)}) custom-call(bf16[512,2048]{1,0:T(8,128)(2,1)} %rows_ref.1, f32[1,2048]{1,0:T(1,128)} %bitcast.15, s32[2,512]{1,0:T(2,128)} %routes_ref.3, bf16[512,128]{1,0:T(8,128)(2,1)} %key_ref.1, bf16[512,128]{1,0:T(8,128)(2,1)} %value_ref.1, f32[1,128]{1,0:T(1,128)} %bitcast.17), custom_call_target="tpu_custom_call" | custom-call | tf_op jit(solution)/shard_map/prologue/pallas_call | solution.py:689
  7.2 197.1 %spread.1 = (bf16[8,48,2048]{2,1,0:T(8,128)(2,1)}, bf16[32,512,256]{2,1,0:T(8,128)(2,1)}, bf16[4,2048,256]{2,1,0:T(8,128)(2,1)}, bf16[4,2048,256]{2,1,0:T(8,128)...) custom-call(bf16[8,48,2048]{2,1,0:T(8,128)(2,1)} %get-tuple-element.12.send_ref, ...), custom_call_target="tpu_custom_call" | custom-call | tf_op jit(solution)/shard_map/spread/pallas_call | solution.py:710
  204.3 10.9 %experts.1.result_ref = bf16[4,8,48,512]{3,2,1,0:T(8,128)(2,1)} custom-call(bf16[384,2048]{1,0:T(8,128)(2,1)} %bitcast.10, bf16[4,2048,256]{2,1,0:T(8,128)(2,1)} %get-tuple-element.15.gate_ref, bf16[4,2048,256]{2,1,0:T(8,128)(2,1)} %get-tuple-element.16.up_ref, bf16[4,256,2048]{2,1,0:T(8,128)(2,1)} %get-tuple-element.17.down_ref), custom_call_target="tpu_custom_call" | custom-call | tf_op jit(solution)/shard_map/experts/pallas_call | solution.py:748
  215.2 0.0 copy-start
  215.2 6.5 %attention.1.attended_ref = bf16[512,256]{1,0:T(8,128)(2,1)} custom-call(bf16[512,256]{1,0:T(8,128)(2,1)} %query_ref.1, f32[1,128]{1,0:T(1,128)} %bitcast.16, f32[2,16384]{1,0:T(2,128)} %forget_ref.1, bf16[32,512,256]{2,1,0:T(8,128)(2,1)} %get-tuple-element.18.kv_ref), custom_call_target="tpu_custom_call" | custom-call | tf_op jit(solution)/shard_map/attention/pallas_call | solution.py:767
  221.7 134.8 %give_back.1 = (bf16[32,48,512]{2,1,0:T(8,128)(2,1)}, bf16[4,128,256]{2,1,0:T(8,128)(2,1)}) custom-call(bf16[4,8,48,512]{3,2,1,0:T(8,128)(2,1)} %experts.1.result_ref, bf16[512,256]{1,0:T(8,128)(2,1)} %attention.1.attended_ref), custom_call_target="tpu_custom_call" | custom-call | tf_op jit(solution)/shard_map/give_back/pallas_call | solution.py:782
  356.5 0.0 copy-done
  356.5 0.9 copy.16
  357.4 6.3 %combine.1 = (bf16[128,2048]{1,0:T(8,128)(2,1)}, bf16[512,512]{1,0:T(8,128)(2,1)}) custom-call(bf16[1536,512]{1,0:T(8,128)(2,1)} %bitcast.9, s32[2,512]{1,0:T(2,128)} %routes_ref.3, f32[512,2]{1,0:T(8,128)} %bitcast.14, bf16[4,128,256]{2,1,0:T(8,128)(2,1)} %get-tuple-element.20.heads_ref, bf16[4,256,2048]{2,1,0:T(8,128)(2,1)} %get-tuple-element.21.out_w_ref), custom_call_target="tpu_custom_call" | custom-call | tf_op jit(solution)/shard_map/combine/pallas_call | solution.py:801
Async XLA Ops:
  215.2 141.4 %copy-start = (f32[2,512]{1,0:T(2,128)S(1)}, f32[2,512]{1,0:T(2,128)}, u32[]{:S(2)}) copy-start(f32[2,512]{1,0:T(2,128)} %param.24) | copy-start | bytes 12292

commit v2 on v1

v2 whole, which is shorter than its diff:
```python
import functools

import jax
import jax.numpy as jnp
from jax import lax
from jax.experimental import pallas as pl
from jax.experimental.pallas import tpu as pltpu
from jax.sharding import PartitionSpec as P

HEAD_SIZE = 128
EXPERTS = 32
CAP = 48
TOP = 2
CORES = 2
LOG2E = 1.4426950408889634
MESH = pl.DeviceIdType.MESH
F32 = jnp.float32
BF16 = jnp.bfloat16


def dot(a, b, dims=(((1,), (0,)), ((), ()))):
    return lax.dot_general(a, b, dims, preferred_element_type=F32)


def row_norm(rows, gain):
    wide = rows.astype(F32)
    factor = lax.rsqrt(jnp.mean(wide * wide, axis=-1, keepdims=True) + 1e-06)
    return wide * factor * gain


def member_and_rank(routes, expert_col):
    tokens = routes.shape[1]
    count = expert_col.shape[0]
    named = jnp.logical_or(routes[0:1, :] == expert_col, routes[1:2, :] == expert_col)
    member = jnp.where(named, 1.0, 0.0).astype(F32)
    before = lax.broadcasted_iota(jnp.int32, (tokens, tokens), 0)
    after = lax.broadcasted_iota(jnp.int32, (tokens, tokens), 1)
    earlier = jnp.where(before < after, 1.0, 0.0).astype(BF16)
    del count
    return member, dot(member.astype(BF16), earlier)


def prologue_kernel(
    n_tp,
    rows_ref,
    gain_ref,
    routes_ref,
    key_ref,
    value_ref,
    key_gain_ref,
    send_ref,
    own_key_ref,
    own_value_ref,
    normed,
):
    span = rows_ref.shape[0]
    me, t = lax.axis_index("ep"), lax.axis_index("tp")
    offset = lax.rem(t + (n_tp - 1) * me, n_tp)
    own_key_ref[...] = row_norm(key_ref[...], key_gain_ref[...]).astype(BF16)
    own_value_ref[...] = value_ref[...].astype(F32).T.astype(BF16)
    step = 64
    for first in range(0, span, step):
        normed[first : first + step, :] = row_norm(
            rows_ref[first : first + step, :], gain_ref[...]
        ).astype(BF16)
    here = EXPERTS // n_tp
    expert_col = offset + n_tp * lax.broadcasted_iota(jnp.int32, (here, 1), 0)
    member, rank = member_and_rank(routes_ref[...], expert_col)
    place = jnp.where(member > 0.5, rank, -1.0)
    slot = lax.broadcasted_iota(jnp.int32, (CAP, span), 0).astype(F32)
    for m in range(here):
        pick = jnp.where(place[m : m + 1, :] == slot, 1.0, 0.0).astype(BF16)
        send_ref[m] = dot(pick, normed[...]).astype(BF16)


def split_three(value):
    high = value.astype(BF16)
    rest = value - high.astype(F32)
    mid = rest.astype(BF16)
    low = (rest - mid.astype(F32)).astype(BF16)
    return high.astype(F32), mid.astype(F32), low.astype(F32)


def prepare_attention(
    heads, blocks, query_ref, gain_ref, forget_ref, query_t, bias, run_max, run_sum, acc
):
    span = query_ref.shape[0]
    columns = heads * span
    for h in range(heads):
        normed = row_norm(query_ref[:, h * HEAD_SIZE : (h + 1) * HEAD_SIZE], gain_ref[...])
        rounded = normed.astype(BF16).astype(F32)
        query_t[:HEAD_SIZE, h * span : (h + 1) * span] = rounded.T.astype(BF16)
    row = lax.broadcasted_iota(jnp.int32, (HEAD_SIZE, columns), 0)
    head = lax.broadcasted_iota(jnp.int32, (HEAD_SIZE, columns), 1) // span
    query_t[HEAD_SIZE:, :] = jnp.where(row // 3 == head, 1.0, 0.0).astype(BF16)
    run_max[...] = jnp.full(run_max.shape, -1e30, F32)
    run_sum[...] = jnp.zeros(run_sum.shape, F32)
    acc[...] = jnp.zeros(acc.shape, F32)
    lane = lax.broadcasted_iota(jnp.int32, (8, HEAD_SIZE), 1)
    sub = lax.broadcasted_iota(jnp.int32, (8, HEAD_SIZE), 0)
    place = jnp.where(lane == sub, 1.0, 0.0).astype(BF16)

    def one(block, carry):
        first = pl.multiple_of(block * span, span)
        rows = []
        for h in range(heads):
            gates = forget_ref[h : h + 1, pl.ds(first, span)]
            rows.extend(split_three(gates * (-(HEAD_SIZE**0.5))))
        rows.append(jnp.zeros((8 - len(rows), span), F32))
        stacked = jnp.concatenate(rows, axis=0).astype(BF16)
        bias[block] = dot(stacked, place, (((0,), (0,)), ((), ()))).astype(BF16)
        return carry

    lax.fori_loop(0, blocks, one, 0)


def attend_block(block, masked, keys_all, values_all, query_t, bias, run_max, run_sum, acc):
    span = keys_all.shape[1]
    columns = query_t.shape[1]
    exp_scale = HEAD_SIZE ** (-0.5) * LOG2E
    width = 256
    keys = jnp.concatenate([keys_all[block], bias[block]], axis=1)
    values = values_all[block]
    for first_col in range(0, columns, width):
        cols = slice(first_col, first_col + width)
        scores = dot(keys, query_t[:, cols])
        if masked:
            key_at = lax.broadcasted_iota(jnp.int32, (span, width), 0)
            query_at = lax.broadcasted_iota(jnp.int32, (span, width), 1) + first_col % span
            scores = jnp.where(key_at <= query_at, scores, -1e30)
        old_max = run_max[:, cols]
        new_max = jnp.maximum(old_max, jnp.max(scores, axis=0, keepdims=True))
        shrink = jnp.exp2((old_max - new_max) * exp_scale)
        weights = jnp.exp2((scores - new_max) * exp_scale)
        run_max[:, cols] = new_max
        run_sum[:, cols] = shrink * run_sum[:, cols] + jnp.sum(weights, axis=0, keepdims=True)
        acc[:, cols] = shrink * acc[:, cols] + dot(values, weights.astype(BF16))


def finish_attention(heads, out_ref, run_sum, acc):
    span = out_ref.shape[0]
    for h in range(heads):
        cols = slice(h * span, (h + 1) * span)
        attended = (acc[:, cols] / run_sum[:, cols]).T
        out_ref[:, h * HEAD_SIZE : (h + 1) * HEAD_SIZE] = attended.astype(BF16)


def remote(src, dst, send_sem, recv_sem, where):
    return pltpu.make_async_remote_copy(
        src_ref=src,
        dst_ref=dst,
        send_sem=send_sem,
        recv_sem=recv_sem,
        device_id=where,
        device_id_type=MESH,
    )


def spread_kernel(
    n_ep,
    n_tp,
    heads,
    send_ref,
    key_ref,
    value_ref,
    query_ref,
    query_gain_ref,
    forget_ref,
    gate_ref,
    up_ref,
    down_ref,
    recv_ref,
    gate_all,
    up_all,
    down_all,
    attended_ref,
    keys_all,
    values_all,
    query_t,
    bias,
    run_max,
    run_sum,
    acc,
    gate_own,
    up_own,
    down_own,
    row_own,
    row_send,
    row_recv,
    fwd_send,
    fwd_recv,
    bwd_send,
    bwd_recv,
    core_send,
    core_recv,
    side_send,
    side_recv,
    half_send,
    half_recv,
    local,
):
    me, t = lax.axis_index("ep"), lax.axis_index("tp")
    n_z = n_ep // CORES
    z, core = me // CORES, lax.rem(me, CORES)
    offset = lax.rem(t + (n_tp - 1) * me, n_tp)
    here = n_ep // n_tp
    right, left = lax.rem(t + 1, n_tp), lax.rem(t + n_tp - 1, n_tp)
    up_ep = CORES * lax.rem(z + 1, n_z) + core
    down_ep = CORES * lax.rem(z + n_z - 1, n_z) + core
    other = CORES * z + (1 - core)
    reach = n_z // 2
    self_slot = me // n_tp
    is_self = lax.rem(me, n_tp) == offset

    barrier = pltpu.get_barrier_semaphore()
    for where in (
        {"ep": up_ep},
        {"ep": down_ep},
        {"ep": other},
        {"tp": right},
        {"tp": left},
    ):
        pl.semaphore_signal(barrier, inc=1, device_id=where, device_id_type=MESH)
    for m in range(here):
        mate = offset + n_tp * m

        @pl.when(mate != me)
        def _(mate=mate):
            pl.semaphore_signal(barrier, inc=1, device_id={"ep": mate}, device_id_type=MESH)

    pl.semaphore_wait(barrier, 5 + here - jnp.where(is_self, 1, 0))

    weights = (
        (gate_ref, gate_all, gate_own),
        (up_ref, up_all, up_own),
        (down_ref, down_all, down_own),
    )

    def side_copy(a, way):
        where = {"tp": (right, left)[way]}
        return remote(
            weights[a][0], weights[a][1].at[t], side_send.at[a, way], side_recv.at[a, way], where
        )

    def half_copy(a, way):
        where = {"tp": (right, left)[way]}
        owner = (left, right)[way]
        full = weights[a][1]
        half = full.shape[1] // 2
        part = full.at[owner, pl.ds(way * half, half)]
        return remote(part, part, half_send.at[a, way], half_recv.at[a, way], where)

    def hand_on(a):
        for way in range(2):
            side_copy(a, way).wait_recv()
            half_copy(a, way).start()

    own = [
        (
            pltpu.make_async_copy(src, held, local.at[a]),
            pltpu.make_async_copy(held, full.at[t], local.at[a]),
        )
        for a, (src, full, held) in enumerate(weights)
    ]
    own_row = (
        pltpu.make_async_copy(send_ref.at[self_slot], row_own, local.at[3]),
        pltpu.make_async_copy(row_own, recv_ref.at[self_slot], local.at[3]),
    )

    def block_copy(part, source_z, source_core, send_sem, recv_sem, where, mine=False):
        block = (keys_all, values_all)[part].at[CORES * source_z + source_core]
        return remote((key_ref, value_ref)[part] if mine else block, block, send_sem, recv_sem, where)

    def fwd_copy(s, part):
        source = lax.rem(z - s + n_z, n_z)
        sems = fwd_send.at[s, part], fwd_recv.at[s, part]
        return block_copy(part, source, core, *sems, {"ep": up_ep}, s == 0)

    def fwd_arrival(s, part):
        source = lax.rem(z - 1 - s + n_z, n_z)
        sems = fwd_send.at[s, part], fwd_recv.at[s, part]
        return block_copy(part, source, core, *sems, {"ep": up_ep})

    def bwd_copy(s, part):
        sems = bwd_send.at[s, part], bwd_recv.at[s, part]
        return block_copy(part, lax.rem(z + s, n_z), core, *sems, {"ep": down_ep}, s == 0)

    def bwd_arrival(s, part):
        sems = bwd_send.at[s, part], bwd_recv.at[s, part]
        return block_copy(part, lax.rem(z + 1 + s, n_z), core, *sems, {"ep": down_ep})

    def core_copy(k, part, source_z, source_core, mine=False):
        sems = core_send.at[k, part], core_recv.at[k, part]
        return block_copy(part, source_z, source_core, *sems, {"ep": other}, mine)

    def core_fwd(s, part, source_core):
        return core_copy(1 + s, part, lax.rem(z - 1 - s + n_z, n_z), source_core)

    def core_bwd(s, part, source_core):
        return core_copy(1 + reach + s, part, lax.rem(z + 1 + s, n_z), source_core)

    def fwd_sends(s):
        return jnp.logical_and(z - s >= 0, z + 1 <= n_z - 1)

    def fwd_gets(s):
        return z - 1 - s >= 0

    def bwd_sends(s):
        return lax.rem(z + s, n_z) <= reach - 2

    def bwd_gets(s):
        return lax.rem(z + 1 + s, n_z) <= reach - 2

    def bwd_needed(s):
        return jnp.logical_and(bwd_gets(s), lax.rem(z + 1 + s, n_z) < z)

    def row_copy(k):
        m = lax.rem(self_slot + k, here)
        mate = offset + n_tp * m
        return mate, remote(
            send_ref.at[m],
            recv_ref.at[self_slot],
            row_send.at[m],
            row_recv.at[self_slot],
            {"ep": mate},
        )

    for a in range(3):
        for way in range(2):
            side_copy(a, way).start()

    for part in range(2):

        @pl.when(fwd_sends(0))
        def _(part=part):
            fwd_copy(0, part).start()

        @pl.when(bwd_sends(0))
        def _(part=part):
            bwd_copy(0, part).start()

        @pl.when(core == 0)
        def _(part=part):
            core_copy(0, part, z, 0, True).start()

    for copies in own:
        copies[0].start()

    @pl.when(is_self)
    def _():
        own_row[0].start()

    keys_all[me] = key_ref[...]
    values_all[me] = value_ref[...]
    prepare_attention(
        heads, me + 1, query_ref, query_gain_ref, forget_ref, query_t, bias, run_max, run_sum, acc
    )
    for copies in own:
        copies[0].wait()
        copies[1].start()

    @pl.when(is_self)
    def _():
        own_row[0].wait()
        own_row[1].start()

    for s in range(reach):
        for part in range(2):

            @pl.when(fwd_gets(s))
            def _(s=s, part=part):
                fwd_arrival(s, part).wait_recv()

            if s + 1 < reach:

                @pl.when(fwd_sends(s + 1))
                def _(s=s, part=part):
                    fwd_copy(s + 1, part).start()

            @pl.when(fwd_gets(s))
            def _(s=s, part=part):
                core_fwd(s, part, core).start()

            if s < reach - 1:

                @pl.when(bwd_gets(s))
                def _(s=s, part=part):
                    bwd_arrival(s, part).wait_recv()

                if s + 1 < reach - 1:

                    @pl.when(bwd_sends(s + 1))
                    def _(s=s, part=part):
                        bwd_copy(s + 1, part).start()

                @pl.when(bwd_needed(s))
                def _(s=s, part=part):
                    core_bwd(s, part, core).start()

        if s == reach // 2:
            hand_on(0)

    for k in range(here):
        mate, copy = row_copy(k)

        @pl.when(mate != me)
        def _(copy=copy):
            copy.start()

    hand_on(1)

    for part in range(2):

        @pl.when(core == 1)
        def _(part=part):
            core_copy(0, part, z, 0).wait_recv()

        for s in range(reach):

            @pl.when(fwd_gets(s))
            def _(s=s, part=part):
                core_fwd(s, part, 1 - core).wait_recv()

            if s < reach - 1:

                @pl.when(bwd_needed(s))
                def _(s=s, part=part):
                    core_bwd(s, part, 1 - core).wait_recv()

    state = (keys_all, values_all, query_t, bias, run_max, run_sum, acc)

    def body(block, carry):
        attend_block(block, False, *state)
        return carry

    middle = me // 2
    lax.fori_loop(0, middle, body, 0)
    hand_on(2)
    lax.fori_loop(middle, me, body, 0)
    attend_block(me, True, *state)
    finish_attention(heads, attended_ref, run_sum, acc)

    for a in range(3):
        for way in range(2):
            side_copy(a, way).wait_send()
            half_copy(a, way).wait_recv()
            half_copy(a, way).wait_send()
    for k in range(here):
        mate, copy = row_copy(k)

        @pl.when(mate != me)
        def _(copy=copy):
            copy.wait_send()

        source = offset + n_tp * k
        arrival = remote(
            send_ref.at[k], recv_ref.at[k], row_send.at[k], row_recv.at[k], {"ep": source}
        )

        @pl.when(source != me)
        def _(arrival=arrival):
            arrival.wait_recv()

    for part in range(2):

        @pl.when(core == 0)
        def _(part=part):
            core_copy(0, part, z, 0, True).wait_send()

        for s in range(reach):

            @pl.when(fwd_sends(s))
            def _(s=s, part=part):
                fwd_copy(s, part).wait_send()

            @pl.when(fwd_gets(s))
            def _(s=s, part=part):
                core_fwd(s, part, core).wait_send()

            if s < reach - 1:

                @pl.when(bwd_sends(s))
                def _(s=s, part=part):
                    bwd_copy(s, part).wait_send()

                @pl.when(bwd_needed(s))
                def _(s=s, part=part):
                    core_bwd(s, part, core).wait_send()

    for copies in own:
        copies[1].wait()

    @pl.when(is_self)
    def _():
        own_row[1].wait()


def expert_kernel(rows_ref, gate_ref, up_ref, down_ref, out_ref, total):
    p = pl.program_id(0)
    parts, sources = out_ref.shape[0], out_ref.shape[1]
    width = out_ref.shape[3]
    rows = rows_ref[...]
    gate = dot(rows, gate_ref[0])
    up = dot(rows, up_ref[0])
    hidden = (gate / (1.0 + jnp.exp(-gate)) * up).astype(BF16)

    @pl.when(p == 0)
    def _():
        total[...] = jnp.zeros(total.shape, F32)

    for q in range(parts):
        cols = slice(q * width, (q + 1) * width)
        piece = dot(hidden, down_ref[0, :, cols]).astype(BF16).astype(F32)
        total[:, cols] += piece

    @pl.when(p == pl.num_programs(0) - 1)
    def _():
        for q in range(parts):
            for n in range(sources):
                out_ref[q, n] = total[
                    n * CAP : (n + 1) * CAP, q * width : (q + 1) * width
                ].astype(BF16)


def return_kernel(
    n_ep,
    n_tp,
    result_ref,
    attended_ref,
    out_ref,
    back_ref,
    heads_ref,
    out_all,
    out_own,
    row_send,
    row_recv,
    head_send,
    head_recv,
    side_send,
    side_recv,
    core_send,
    core_recv,
    local,
):
    me, t = lax.axis_index("ep"), lax.axis_index("tp")
    offset = lax.rem(t + (n_tp - 1) * me, n_tp)
    here = n_ep // n_tp
    token_rows = attended_ref.shape[0] // n_tp
    self_slot = me // n_tp
    is_self = lax.rem(me, n_tp) == offset

    barrier = pltpu.get_barrier_semaphore()
    for e in range(n_ep):
        column = lax.rem(me + e, n_tp)

        @pl.when(jnp.logical_not(jnp.logical_and(me == e, column == t)))
        def _(e=e, column=column):
            pl.semaphore_signal(
                barrier, inc=1, device_id={"ep": e, "tp": column}, device_id_type=MESH
            )

    for k in range(1, n_tp):
        pl.semaphore_signal(
            barrier, inc=1, device_id={"tp": lax.rem(t + k, n_tp)}, device_id_type=MESH
        )
    core = lax.rem(me, CORES)
    other = me + 1 - 2 * core
    right, left = lax.rem(t + 1, n_tp), lax.rem(t + n_tp - 1, n_tp)
    across = lax.rem(t + 2, n_tp)
    pl.semaphore_signal(barrier, inc=1, device_id={"ep": other}, device_id_type=MESH)
    pl.semaphore_wait(barrier, n_ep + n_tp - jnp.where(is_self, 1, 0))

    out_rows = out_ref.shape[0] // CORES
    out_first = core * out_rows
    quarter = out_rows // 2

    def side_copy(way):
        mine = pl.ds(out_first, out_rows)
        where = {"tp": (right, left)[way]}
        return remote(
            out_ref.at[mine], out_all.at[t, mine], side_send.at[0, way], side_recv.at[0, way], where
        )

    def half_copy(way):
        where = {"tp": (right, left)[way]}
        owner = (left, right)[way]
        part = out_all.at[owner, pl.ds(out_first + way * quarter, quarter)]
        return remote(part, part, side_send.at[1, way], side_recv.at[1, way], where)

    def core_copy(k, first):
        part = out_all.at[(left, right, across)[k], pl.ds(first, out_rows)]
        return remote(part, part, core_send.at[k], core_recv.at[k], {"ep": other})

    own_out = (
        pltpu.make_async_copy(out_ref, out_own, local.at[2]),
        pltpu.make_async_copy(out_own, out_all.at[t], local.at[2]),
    )

    def head_copy(k):
        q = lax.rem(t + k, n_tp)
        first = pl.multiple_of(q * token_rows, token_rows)
        return remote(
            attended_ref.at[pl.ds(first, token_rows)],
            heads_ref.at[t],
            head_send.at[k],
            head_recv.at[k],
            {"tp": q},
        )

    own_first = pl.multiple_of(t * token_rows, token_rows)
    own_heads = pltpu.make_async_copy(
        attended_ref.at[pl.ds(own_first, token_rows)], heads_ref.at[t], local.at[0]
    )
    own_row = pltpu.make_async_copy(result_ref.at[t, self_slot], back_ref.at[me], local.at[1])

    def row_copy(k, j):
        n = lax.rem(self_slot + k, here)
        q = lax.rem(t + j, n_tp)
        target = offset + n_tp * n
        away = jnp.logical_not(jnp.logical_and(target == me, q == t))
        return away, remote(
            result_ref.at[q, n],
            back_ref.at[me],
            row_send.at[k, j],
            row_recv.at[me],
            {"ep": target, "tp": q},
        )

    for k in range(1, n_tp):
        head_copy(k).start()
    own_heads.start()

    @pl.when(is_self)
    def _():
        own_row.start()

    for k in range(here):
        for j in range(n_tp):
            away, copy = row_copy(k, j)

            @pl.when(away)
            def _(copy=copy):
                copy.start()

    for way in range(2):
        side_copy(way).start()
    own_out[0].start()
    own_out[0].wait()
    own_out[1].start()
    for way in range(2):
        side_copy(way).wait_recv()
        half_copy(way).start()
        core_copy(way, out_first).start()
    for way in range(2):
        half_copy(way).wait_recv()
    core_copy(2, out_first).start()
    for way in range(2):
        side_copy(way).wait_send()
        half_copy(way).wait_send()
    for k in range(3):
        core_copy(k, out_first).wait_send()
        core_copy(k, (1 - core) * out_rows).wait_recv()
    own_out[1].wait()

    for k in range(here):
        for j in range(n_tp):
            away, copy = row_copy(k, j)

            @pl.when(away)
            def _(copy=copy):
                copy.wait_send()

    for e in range(n_ep):
        column = lax.rem(me + e, n_tp)
        arrival = remote(
            result_ref.at[0, 0],
            back_ref.at[e],
            row_send.at[0, 0],
            row_recv.at[e],
            {"ep": e, "tp": column},
        )

        @pl.when(jnp.logical_not(jnp.logical_and(me == e, column == t)))
        def _(arrival=arrival):
            arrival.wait_recv()

    for k in range(1, n_tp):
        source = lax.rem(t + n_tp - k, n_tp)
        head_copy(k).wait_send()
        remote(
            attended_ref.at[pl.ds(0, token_rows)],
            heads_ref.at[source],
            head_send.at[k],
            head_recv.at[k],
            {"tp": source},
        ).wait_recv()
    own_heads.wait()

    @pl.when(is_self)
    def _():
        own_row.wait()


def combine_kernel(back_ref, routes_ref, weight_ref, heads_ref, out_w_ref, mixer_ref, out_ref):
    slots = back_ref.shape[0]
    span = routes_ref.shape[1]
    expert_col = lax.broadcasted_iota(jnp.int32, (EXPERTS, 1), 0)
    routes = routes_ref[...]
    _, rank = member_and_rank(routes, expert_col)
    total = None
    for j in range(TOP):
        chosen = routes[j : j + 1, :]
        within = jnp.sum(jnp.where(chosen == expert_col, rank, 0.0), axis=0, keepdims=True)
        slot = chosen * CAP + within.astype(jnp.int32)
        at = lax.broadcasted_iota(jnp.int32, (slots, span), 0)
        pick = jnp.where(at == slot, 1.0, 0.0).astype(BF16)
        picked = dot(pick, back_ref[...], (((0,), (0,)), ((), ())))
        term = picked * weight_ref[:, j : j + 1]
        total = term if total is None else total + term
    out_ref[...] = total.astype(BF16)
    projected = None
    for k in range(heads_ref.shape[0]):
        piece = dot(heads_ref[k], out_w_ref[k])
        projected = piece if projected is None else projected + piece
    mixer_ref[...] = projected.astype(BF16)


def on_device(
    n_ep,
    n_tp,
    queries,
    key_rows,
    value_rows,
    query_gain,
    key_gain,
    log_forget,
    out_weight,
    expert_rows,
    expert_gain,
    routes,
    route_weight,
    gate_weight,
    up_weight,
    down_weight,
):
    span, model_width = expert_rows.shape
    here = n_ep // n_tp
    heads = queries.shape[1] // HEAD_SIZE
    width = model_width // n_tp
    n_z = n_ep // CORES
    reach = n_z // 2
    ff_part = gate_weight.shape[2]
    hbm = pl.BlockSpec(memory_space=pltpu.HBM)
    vmem = pl.BlockSpec(memory_space=pltpu.VMEM)
    shape = jax.ShapeDtypeStruct
    big = pltpu.CompilerParams(vmem_limit_bytes=56 * 1024 * 1024)

    send_rows, own_keys, own_values = pl.pallas_call(
        functools.partial(prologue_kernel, n_tp),
        out_shape=(
            shape((here, CAP, model_width), BF16),
            shape((span, HEAD_SIZE), BF16),
            shape((HEAD_SIZE, span), BF16),
        ),
        in_specs=[vmem] * 6,
        out_specs=(vmem,) * 3,
        scratch_shapes=[pltpu.VMEM((span, model_width), BF16)],
        compiler_params=big,
        name="prologue",
    )(
        expert_rows,
        expert_gain.reshape(1, -1),
        routes,
        key_rows,
        value_rows,
        key_gain.reshape(1, -1),
    )

    dma = pltpu.SemaphoreType.DMA
    columns = heads * span
    recv_rows, gate_all, up_all, down_all, attended = pl.pallas_call(
        functools.partial(spread_kernel, n_ep, n_tp, heads),
        out_shape=(
            shape((here, CAP, model_width), BF16),
            shape((n_tp, model_width, ff_part), BF16),
            shape((n_tp, model_width, ff_part), BF16),
            shape((n_tp, ff_part, model_width), BF16),
            shape((span, columns // span * HEAD_SIZE), BF16),
        ),
        in_specs=[hbm] + [vmem] * 5 + [hbm] * 3,
        out_specs=(hbm,) * 4 + (vmem,),
        scratch_shapes=[
            pltpu.VMEM((n_ep, span, HEAD_SIZE), BF16),
            pltpu.VMEM((n_ep, HEAD_SIZE, span), BF16),
            pltpu.VMEM((2 * HEAD_SIZE, columns), BF16),
            pltpu.VMEM((n_ep, span, HEAD_SIZE), BF16),
            pltpu.VMEM((1, columns), F32),
            pltpu.VMEM((1, columns), F32),
            pltpu.VMEM((HEAD_SIZE, columns), F32),
            pltpu.VMEM((model_width, ff_part), BF16),
            pltpu.VMEM((model_width, ff_part), BF16),
            pltpu.VMEM((ff_part, model_width), BF16),
            pltpu.VMEM((CAP, model_width), BF16),
            dma((here,)),
            dma((here,)),
            dma((reach, 2)),
            dma((reach, 2)),
            dma((reach - 1, 2)),
            dma((reach - 1, 2)),
            dma((2 * reach, 2)),
            dma((2 * reach, 2)),
            dma((3, 2)),
            dma((3, 2)),
            dma((3, 2)),
            dma((3, 2)),
            dma((4,)),
        ],
        compiler_params=pltpu.CompilerParams(
            collective_id=0, has_side_effects=True, vmem_limit_bytes=56 * 1024 * 1024
        ),
        name="spread",
    )(
        send_rows,
        own_keys,
        own_values,
        queries,
        query_gain.reshape(1, -1),
        log_forget,
        gate_weight.reshape(model_width, ff_part),
        up_weight.reshape(model_width, ff_part),
        down_weight.reshape(ff_part, model_width),
    )

    results = pl.pallas_call(
        expert_kernel,
        grid=(n_tp,),
        out_shape=shape((n_tp, here, CAP, width), BF16),
        in_specs=[
            pl.BlockSpec((here * CAP, model_width), lambda p: (0, 0)),
            pl.BlockSpec((1, model_width, ff_part), lambda p: (p, 0, 0)),
            pl.BlockSpec((1, model_width, ff_part), lambda p: (p, 0, 0)),
            pl.BlockSpec((1, ff_part, model_width), lambda p: (p, 0, 0)),
        ],
        out_specs=pl.BlockSpec((n_tp, here, CAP, width), lambda p: (0, 0, 0, 0)),
        scratch_shapes=[pltpu.VMEM((here * CAP, model_width), F32)],
        compiler_params=pltpu.CompilerParams(
            dimension_semantics=("arbitrary",), vmem_limit_bytes=56 * 1024 * 1024
        ),
        name="experts",
    )(recv_rows.reshape(here * CAP, model_width), gate_all, up_all, down_all)

    back_rows, head_rows, out_all = pl.pallas_call(
        functools.partial(return_kernel, n_ep, n_tp),
        out_shape=(
            shape((n_ep, CAP, width), BF16),
            shape((n_tp, span // n_tp, heads * HEAD_SIZE), BF16),
            shape((n_tp, *out_weight.shape), BF16),
        ),
        in_specs=[hbm] * 3,
        out_specs=(hbm,) * 3,
        scratch_shapes=[
            pltpu.VMEM(out_weight.shape, BF16),
            dma((here, n_tp)),
            dma((n_ep,)),
            dma((n_tp,)),
            dma((n_tp,)),
            dma((2, 2)),
            dma((2, 2)),
            dma((3,)),
            dma((3,)),
            dma((3,)),
        ],
        compiler_params=pltpu.CompilerParams(collective_id=1, has_side_effects=True),
        name="give_back",
    )(results, attended, out_weight)

    mixer_out, expert_out = pl.pallas_call(
        combine_kernel,
        out_shape=(
            shape((span // n_tp, model_width), BF16),
            shape((span, width), BF16),
        ),
        in_specs=[vmem] * 5,
        out_specs=(vmem, vmem),
        compiler_params=big,
        name="combine",
    )(back_rows.reshape(n_ep * CAP, width), routes, route_weight.T, head_rows, out_all)
    return (mixer_out, expert_out)


def solution(mesh):
    in_specs = (
        P(("grp", "ep"), "tp"),
        P(("grp", "ep"), "tp"),
        P(("grp", "ep"), "tp"),
        P(),
        P(),
        P("tp", "grp"),
        P("tp", None),
        P(("grp", "ep"), None),
        P(),
        P(None, ("grp", "ep")),
        P(None, ("grp", "ep")),
        P("ep", None, "tp"),
        P("ep", None, "tp"),
        P("ep", "tp", None),
    )
    out_specs = (P(("grp", "ep", "tp"), None), P(("grp", "ep"), "tp"))
    return jax.shard_map(
        functools.partial(on_device, mesh.shape["ep"], mesh.shape["tp"]),
        mesh=mesh,
        in_specs=in_specs,
        out_specs=out_specs,
        check_vma=False,
    )
```

time: 364 us -> 286 us (0.79)
  Pallas kernels: 362 us -> 281 us
    pallas_call x2 -> x1, Pallas kernels: 204 us -> 158 us  [on_device(): pl.pallas_call(functools.partial(spread_kernel, n_ep, n_tp, heads), out_s...]
    pallas_call x1, Pallas kernels: 135 us -> 99.5 us  [on_device(): pl.pallas_call(functools.partial(return_kernel, n_ep, n_tp), out_shape=(s...]
where the time goes in v2:
time: 286 us; the launch traced here: 283 us
  Pallas kernels  281 us (98%)
    pallas_call x1, Pallas kernels, on_device(): pl.pallas_call(functools.partial(spread_kernel, n_ep, n_tp, heads), out_s...  158 us
    pallas_call x1, Pallas kernels, on_device(): pl.pallas_call(functools.partial(return_kernel, n_ep, n_tp), out_shape=(s...  99.5 us
    pallas_call x1, Pallas kernels, on_device(): pl.pallas_call(expert_kernel, grid=(n_tp,), out_shape=shape((n_tp, here,...  11 us
    pallas_call x1, Pallas kernels, on_device(): pl.pallas_call(functools.partial(prologue_kernel, n_tp), out_shape=(shape...  6.57 us
    pallas_call x1, Pallas kernels, on_device(): pl.pallas_call(combine_kernel, out_shape=(shape((span // n_tp, model_widt...  6.28 us

profile of v2, /device:TPU:46, one launch (start us, length us, event | category | flops | bytes accessed | tf_op | source)
XLA Modules:
  0.0 282.8 jit_solution(3790291678491469748)
XLA Ops:
  0.6 6.6 %prologue.1 = (bf16[8,48,2048]{2,1,0:T(8,128)(2,1)}, bf16[512,128]{1,0:T(8,128)(2,1)}, bf16[128,512]{1,0:T(8,128)(2,1)}) custom-call(bf16[512,2048]{1,0:T(8,128)(2,1)} %rows_ref.1, f32[1,2048]{1,0:T(1,128)} %bitcast.15, s32[2,512]{1,0:T(2,128)} %routes_ref.3, bf16[512,128]{1,0:T(8,128)(2,1)} %key_ref.1, bf16[512,128]{1,0:T(8,128)(2,1)} %value_ref.1, ...), custom_call_target="tpu_custom_call" | custom-call | tf_op jit(solution)/shard_map/prologue/pallas_call | solution.py:758
  7.2 158.0 %spread.1 = (bf16[8,48,2048]{2,1,0:T(8,128)(2,1)}, bf16[4,2048,256]{2,1,0:T(8,128)(2,1)}, bf16[4,2048,256]{2,1,0:T(8,128)(2,1)}, bf16[4,256,2048]{2,1,0:T(8,128)(2,1)}, bf16[512,256]{1,0:T(8,128)(2,1)}) custom-call(bf16[8,48,2048]{2,1,0:T(8,128)(2,1)} %get-tuple-element.13.send_ref, bf16[512,128]{1,0:T(8,128)(2,1)} %get-tuple-element.14.key_ref, ...), custom_call_target="tpu_custom_call" | custom-call | tf_op jit(solution)/shard_map/spread/pallas_call | solution.py:781
  165.2 11.0 %experts.1.result_ref = bf16[4,8,48,512]{3,2,1,0:T(8,128)(2,1)} custom-call(bf16[384,2048]{1,0:T(8,128)(2,1)} %bitcast.10, bf16[4,2048,256]{2,1,0:T(8,128)(2,1)} %get-tuple-element.17.gate_ref, bf16[4,2048,256]{2,1,0:T(8,128)(2,1)} %get-tuple-element.18.up_ref, bf16[4,256,2048]{2,1,0:T(8,128)(2,1)} %get-tuple-element.19.down_ref), custom_call_target="tpu_custom_call" | custom-call | tf_op jit(solution)/shard_map/experts/pallas_call | solution.py:834
  176.1 0.0 copy-start
  176.1 99.5 %give_back.1 = (bf16[32,48,512]{2,1,0:T(8,128)(2,1)}, bf16[4,128,256]{2,1,0:T(8,128)(2,1)}, bf16[4,256,2048]{2,1,0:T(8,128)(2,1)}) custom-call(bf16[4,8,48,512]{3,2,1,0:T(8,128)(2,1)} %experts.1.result_ref, bf16[512,256]{1,0:T(8,128)(2,1)} %get-tuple-element.20.attended_ref, bf16[256,2048]{1,0:T(8,128)(2,1)} %out_ref.1), custom_call_target="tpu_custom_call" | custom-call | tf_op jit(solution)/shard_map/give_back/pallas_call | solution.py:852
  275.6 0.0 copy-done
  275.6 0.9 copy.16
  276.5 6.3 %combine.1 = (bf16[128,2048]{1,0:T(8,128)(2,1)}, bf16[512,512]{1,0:T(8,128)(2,1)}) custom-call(bf16[1536,512]{1,0:T(8,128)(2,1)} %bitcast.9, s32[2,512]{1,0:T(2,128)} %routes_ref.3, f32[512,2]{1,0:T(8,128)} %bitcast.14, bf16[4,128,256]{2,1,0:T(8,128)(2,1)} %get-tuple-element.22.heads_ref, bf16[4,256,2048]{2,1,0:T(8,128)(2,1)} %get-tuple-element.23.out_w_ref), custom_call_target="tpu_custom_call" | custom-call | tf_op jit(solution)/shard_map/combine/pallas_call | solution.py:877
Async XLA Ops:
  176.1 99.5 %copy-start = (f32[2,512]{1,0:T(2,128)S(1)}, f32[2,512]{1,0:T(2,128)}, u32[]{:S(2)}) copy-start(f32[2,512]{1,0:T(2,128)} %param.24) | copy-start | bytes 12292

commit v3 on v2

v3 whole, which is shorter than its diff:
```python
import functools

import jax
import jax.numpy as jnp
from jax import lax
from jax.experimental import pallas as pl
from jax.experimental.pallas import tpu as pltpu
from jax.sharding import PartitionSpec as P

HEAD_SIZE = 128
EXPERTS = 32
CAP = 48
TOP = 2
CORES = 2
LOG2E = 1.4426950408889634
MESH = pl.DeviceIdType.MESH
F32 = jnp.float32
BF16 = jnp.bfloat16


def dot(a, b, dims=(((1,), (0,)), ((), ()))):
    return lax.dot_general(a, b, dims, preferred_element_type=F32)


def row_norm(rows, gain):
    wide = rows.astype(F32)
    factor = lax.rsqrt(jnp.mean(wide * wide, axis=-1, keepdims=True) + 1e-06)
    return wide * factor * gain


def member_and_rank(routes, expert_col):
    tokens = routes.shape[1]
    count = expert_col.shape[0]
    named = jnp.logical_or(routes[0:1, :] == expert_col, routes[1:2, :] == expert_col)
    member = jnp.where(named, 1.0, 0.0).astype(F32)
    before = lax.broadcasted_iota(jnp.int32, (tokens, tokens), 0)
    after = lax.broadcasted_iota(jnp.int32, (tokens, tokens), 1)
    earlier = jnp.where(before < after, 1.0, 0.0).astype(BF16)
    del count
    return member, dot(member.astype(BF16), earlier)


def prologue_kernel(
    n_tp,
    rows_ref,
    gain_ref,
    routes_ref,
    key_ref,
    value_ref,
    key_gain_ref,
    send_ref,
    own_key_ref,
    own_value_ref,
    normed,
):
    span = rows_ref.shape[0]
    me, t = lax.axis_index("ep"), lax.axis_index("tp")
    offset = lax.rem(t + (n_tp - 1) * me, n_tp)
    own_key_ref[...] = row_norm(key_ref[...], key_gain_ref[...]).astype(BF16)
    own_value_ref[...] = value_ref[...].astype(F32).T.astype(BF16)
    step = 64
    for first in range(0, span, step):
        normed[first : first + step, :] = row_norm(
            rows_ref[first : first + step, :], gain_ref[...]
        ).astype(BF16)
    here = EXPERTS // n_tp
    expert_col = offset + n_tp * lax.broadcasted_iota(jnp.int32, (here, 1), 0)
    member, rank = member_and_rank(routes_ref[...], expert_col)
    place = jnp.where(member > 0.5, rank, -1.0)
    slot = lax.broadcasted_iota(jnp.int32, (CAP, span), 0).astype(F32)
    for m in range(here):
        pick = jnp.where(place[m : m + 1, :] == slot, 1.0, 0.0).astype(BF16)
        send_ref[m] = dot(pick, normed[...]).astype(BF16)


def split_three(value):
    high = value.astype(BF16)
    rest = value - high.astype(F32)
    mid = rest.astype(BF16)
    low = (rest - mid.astype(F32)).astype(BF16)
    return high.astype(F32), mid.astype(F32), low.astype(F32)


def prepare_attention(
    heads, blocks, query_ref, gain_ref, forget_ref, query_t, bias, run_max, run_sum, acc
):
    span = query_ref.shape[0]
    columns = heads * span
    for h in range(heads):
        normed = row_norm(query_ref[:, h * HEAD_SIZE : (h + 1) * HEAD_SIZE], gain_ref[...])
        rounded = normed.astype(BF16).astype(F32)
        query_t[:HEAD_SIZE, h * span : (h + 1) * span] = rounded.T.astype(BF16)
    row = lax.broadcasted_iota(jnp.int32, (HEAD_SIZE, columns), 0)
    head = lax.broadcasted_iota(jnp.int32, (HEAD_SIZE, columns), 1) // span
    query_t[HEAD_SIZE:, :] = jnp.where(row // 3 == head, 1.0, 0.0).astype(BF16)
    run_max[...] = jnp.full(run_max.shape, -1e30, F32)
    run_sum[...] = jnp.zeros(run_sum.shape, F32)
    acc[...] = jnp.zeros(acc.shape, F32)
    lane = lax.broadcasted_iota(jnp.int32, (8, HEAD_SIZE), 1)
    sub = lax.broadcasted_iota(jnp.int32, (8, HEAD_SIZE), 0)
    place = jnp.where(lane == sub, 1.0, 0.0).astype(BF16)

    def one(block, carry):
        first = pl.multiple_of(block * span, span)
        rows = []
        for h in range(heads):
            gates = forget_ref[h : h + 1, pl.ds(first, span)]
            rows.extend(split_three(gates * (-(HEAD_SIZE**0.5))))
        rows.append(jnp.zeros((8 - len(rows), span), F32))
        stacked = jnp.concatenate(rows, axis=0).astype(BF16)
        bias[block] = dot(stacked, place, (((0,), (0,)), ((), ()))).astype(BF16)
        return carry

    lax.fori_loop(0, blocks, one, 0)


def attend_block(block, masked, keys_all, values_all, query_t, bias, run_max, run_sum, acc):
    span = keys_all.shape[1]
    columns = query_t.shape[1]
    exp_scale = HEAD_SIZE ** (-0.5) * LOG2E
    width = 256
    keys = jnp.concatenate([keys_all[block], bias[block]], axis=1)
    values = values_all[block]
    for first_col in range(0, columns, width):
        cols = slice(first_col, first_col + width)
        scores = dot(keys, query_t[:, cols])
        if masked:
            key_at = lax.broadcasted_iota(jnp.int32, (span, width), 0)
            query_at = lax.broadcasted_iota(jnp.int32, (span, width), 1) + first_col % span
            scores = jnp.where(key_at <= query_at, scores, -1e30)
        old_max = run_max[:, cols]
        new_max = jnp.maximum(old_max, jnp.max(scores, axis=0, keepdims=True))
        shrink = jnp.exp2((old_max - new_max) * exp_scale)
        weights = jnp.exp2((scores - new_max) * exp_scale)
        run_max[:, cols] = new_max
        run_sum[:, cols] = shrink * run_sum[:, cols] + jnp.sum(weights, axis=0, keepdims=True)
        acc[:, cols] = shrink * acc[:, cols] + dot(values, weights.astype(BF16))


def finish_attention(heads, out_ref, run_sum, acc):
    span = out_ref.shape[0]
    for h in range(heads):
        cols = slice(h * span, (h + 1) * span)
        attended = (acc[:, cols] / run_sum[:, cols]).T
        out_ref[:, h * HEAD_SIZE : (h + 1) * HEAD_SIZE] = attended.astype(BF16)


def remote(src, dst, send_sem, recv_sem, where):
    return pltpu.make_async_remote_copy(
        src_ref=src,
        dst_ref=dst,
        send_sem=send_sem,
        recv_sem=recv_sem,
        device_id=where,
        device_id_type=MESH,
    )


def layer_kernel(
    n_ep,
    n_tp,
    heads,
    send_ref,
    key_ref,
    value_ref,
    query_ref,
    query_gain_ref,
    forget_ref,
    gate_ref,
    up_ref,
    down_ref,
    out_ref,
    back_ref,
    heads_ref,
    out_all,
    rows_all,
    total,
    result,
    attended,
    keys_all,
    values_all,
    query_t,
    bias,
    run_max,
    run_sum,
    acc,
    gate_all,
    up_all,
    down_all,
    out_own,
    row_send,
    row_recv,
    fwd_send,
    fwd_recv,
    bwd_send,
    bwd_recv,
    core_send,
    core_recv,
    side_send,
    side_recv,
    half_send,
    half_recv,
    part_send,
    part_recv,
    back_send,
    back_recv,
    head_send,
    head_recv,
    local,
):
    me, t = lax.axis_index("ep"), lax.axis_index("tp")
    n_z = n_ep // CORES
    z, core = me // CORES, lax.rem(me, CORES)
    offset = lax.rem(t + (n_tp - 1) * me, n_tp)
    here = n_ep // n_tp
    right, left = lax.rem(t + 1, n_tp), lax.rem(t + n_tp - 1, n_tp)
    across = lax.rem(t + 2, n_tp)
    up_ep = CORES * lax.rem(z + 1, n_z) + core
    down_ep = CORES * lax.rem(z + n_z - 1, n_z) + core
    other = CORES * z + (1 - core)
    reach = n_z // 2
    self_slot = me // n_tp
    is_self = lax.rem(me, n_tp) == offset
    far_first = [here // 2]
    for k in range(1, here // 2):
        far_first += [here // 2 - k, here // 2 + k]
    far_first.append(0)

    barrier = pltpu.get_barrier_semaphore()
    for where in (
        {"ep": up_ep},
        {"ep": down_ep},
        {"ep": other},
        {"tp": right},
        {"tp": left},
        {"tp": across},
    ):
        pl.semaphore_signal(barrier, inc=1, device_id=where, device_id_type=MESH)
    for m in range(here):
        mate = offset + n_tp * m

        @pl.when(mate != me)
        def _(mate=mate):
            pl.semaphore_signal(barrier, inc=1, device_id={"ep": mate}, device_id_type=MESH)

    def returns_from(e):
        column = lax.rem(me + e, n_tp)
        return column, jnp.logical_not(jnp.logical_and(me == e, column == t))

    for e in range(n_ep):
        column, away = returns_from(e)

        @pl.when(away)
        def _(e=e, column=column):
            pl.semaphore_signal(
                barrier, inc=1, device_id={"ep": e, "tp": column}, device_id_type=MESH
            )

    pl.semaphore_wait(barrier, 6 + here + n_ep - jnp.where(is_self, 2, 0))

    weights = ((gate_ref, gate_all), (up_ref, up_all), (down_ref, down_all))
    out_rows = out_ref.shape[0] // CORES
    out_first = core * out_rows

    def side_copy(a, way):
        where = {"tp": (right, left)[way]}
        if a < 3:
            src, dst = weights[a][0], weights[a][1].at[t]
        else:
            mine = pl.ds(out_first, out_rows)
            src, dst = out_ref.at[mine], out_all.at[t, mine]
        return remote(src, dst, side_send.at[a, way], side_recv.at[a, way], where)

    def half_copy(a, way):
        where = {"tp": (right, left)[way]}
        owner = (left, right)[way]
        if a < 3:
            full = weights[a][1]
            half = full.shape[1] // 2
            part = full.at[owner, pl.ds(way * half, half)]
        else:
            half = out_rows // 2
            part = out_all.at[owner, pl.ds(out_first + way * half, half)]
        return remote(part, part, half_send.at[a, way], half_recv.at[a, way], where)

    def hand_on(a):
        for way in range(2):
            side_copy(a, way).wait_recv()
            half_copy(a, way).start()

    def part_copy(k, first):
        part = out_all.at[(left, right, across)[k], pl.ds(first, out_rows)]
        return remote(part, part, part_send.at[k], part_recv.at[k], {"ep": other})

    own = [
        pltpu.make_async_copy(src, full.at[t], local.at[a])
        for a, (src, full) in enumerate(weights)
    ]
    own_row = pltpu.make_async_copy(
        send_ref.at[self_slot], rows_all.at[self_slot], local.at[3]
    )
    own_out = (
        pltpu.make_async_copy(out_ref, out_own, local.at[4]),
        pltpu.make_async_copy(out_own, out_all.at[t], local.at[4]),
    )

    def row_copy(k):
        m = lax.rem(self_slot + k, here)
        mate = offset + n_tp * m
        return mate, remote(
            send_ref.at[m],
            rows_all.at[self_slot],
            row_send.at[m],
            row_recv.at[self_slot],
            {"ep": mate},
        )

    def row_arrival(n):
        source = offset + n_tp * n
        return source, remote(
            send_ref.at[n], rows_all.at[n], row_send.at[n], row_recv.at[n], {"ep": source}
        )

    def block_copy(part, source_z, source_core, send_sem, recv_sem, where, mine=False):
        block = (keys_all, values_all)[part].at[CORES * source_z + source_core]
        return remote((key_ref, value_ref)[part] if mine else block, block, send_sem, recv_sem, where)

    def fwd_copy(s, part):
        source = lax.rem(z - s + n_z, n_z)
        sems = fwd_send.at[s, part], fwd_recv.at[s, part]
        return block_copy(part, source, core, *sems, {"ep": up_ep}, s == 0)

    def fwd_arrival(s, part):
        source = lax.rem(z - 1 - s + n_z, n_z)
        sems = fwd_send.at[s, part], fwd_recv.at[s, part]
        return block_copy(part, source, core, *sems, {"ep": up_ep})

    def bwd_copy(s, part):
        sems = bwd_send.at[s, part], bwd_recv.at[s, part]
        return block_copy(part, lax.rem(z + s, n_z), core, *sems, {"ep": down_ep}, s == 0)

    def bwd_arrival(s, part):
        sems = bwd_send.at[s, part], bwd_recv.at[s, part]
        return block_copy(part, lax.rem(z + 1 + s, n_z), core, *sems, {"ep": down_ep})

    def core_copy(k, part, source_z, source_core, mine=False):
        sems = core_send.at[k, part], core_recv.at[k, part]
        return block_copy(part, source_z, source_core, *sems, {"ep": other}, mine)

    def core_fwd(s, part, source_core):
        return core_copy(1 + s, part, lax.rem(z - 1 - s + n_z, n_z), source_core)

    def core_bwd(s, part, source_core):
        return core_copy(1 + reach + s, part, lax.rem(z + 1 + s, n_z), source_core)

    def fwd_sends(s):
        return jnp.logical_and(z - s >= 0, z + 1 <= n_z - 1)

    def fwd_gets(s):
        return z - 1 - s >= 0

    def bwd_sends(s):
        return lax.rem(z + s, n_z) <= reach - 2

    def bwd_gets(s):
        return lax.rem(z + 1 + s, n_z) <= reach - 2

    def bwd_needed(s):
        return jnp.logical_and(bwd_gets(s), lax.rem(z + 1 + s, n_z) < z)

    def back_copy(k, j):
        n = lax.rem(self_slot + far_first[k], here)
        q = lax.rem(t + j, n_tp)
        target = offset + n_tp * n
        away = jnp.logical_not(jnp.logical_and(target == me, q == t))
        return away, remote(
            result.at[q, n],
            back_ref.at[me],
            back_send.at[k, j],
            back_recv.at[me],
            {"ep": target, "tp": q},
        )

    own_back = pltpu.make_async_copy(result.at[t, self_slot], back_ref.at[me], local.at[3])

    token_rows = attended.shape[0] // n_tp

    def head_copy(k):
        q = lax.rem(t + k, n_tp)
        first = pl.multiple_of(q * token_rows, token_rows)
        return remote(
            attended.at[pl.ds(first, token_rows)],
            heads_ref.at[t],
            head_send.at[k],
            head_recv.at[k],
            {"tp": q},
        )

    own_heads = pltpu.make_async_copy(
        attended.at[pl.ds(pl.multiple_of(t * token_rows, token_rows), token_rows)],
        heads_ref.at[t],
        local.at[0],
    )

    def expert_part(p, first):
        rows = rows_all[...].reshape(here * CAP, rows_all.shape[2])
        gate = dot(rows, gate_all[p])
        up = dot(rows, up_all[p])
        hidden = (gate / (1.0 + jnp.exp(-gate)) * up).astype(BF16)
        width = result.shape[3]
        for q in range(n_tp):
            cols = slice(q * width, (q + 1) * width)
            piece = dot(hidden, down_all[p, :, cols]).astype(BF16).astype(F32)
            if first:
                total[:, cols] = piece
            else:
                total[:, cols] += piece

    for a in range(3):
        for way in range(2):
            side_copy(a, way).start()

    for k in far_first:
        mate, copy = row_copy(k)

        @pl.when(mate != me)
        def _(copy=copy):
            copy.start()

    for part in range(2):

        @pl.when(fwd_sends(0))
        def _(part=part):
            fwd_copy(0, part).start()

        @pl.when(bwd_sends(0))
        def _(part=part):
            bwd_copy(0, part).start()

        @pl.when(core == 0)
        def _(part=part):
            core_copy(0, part, z, 0, True).start()

    for copy in own:
        copy.start()
    own_out[0].start()

    @pl.when(is_self)
    def _():
        own_row.start()

    keys_all[me] = key_ref[...]
    values_all[me] = value_ref[...]
    prepare_attention(
        heads, me + 1, query_ref, query_gain_ref, forget_ref, query_t, bias, run_max, run_sum, acc
    )
    own_out[0].wait()
    own_out[1].start()
    for copy in own:
        copy.wait()

    hand_on(0)
    for s in range(reach):
        for part in range(2):

            @pl.when(fwd_gets(s))
            def _(s=s, part=part):
                fwd_arrival(s, part).wait_recv()

            if s + 1 < reach:

                @pl.when(fwd_sends(s + 1))
                def _(s=s, part=part):
                    fwd_copy(s + 1, part).start()

            @pl.when(fwd_gets(s))
            def _(s=s, part=part):
                core_fwd(s, part, core).start()

            if s < reach - 1:

                @pl.when(bwd_gets(s))
                def _(s=s, part=part):
                    bwd_arrival(s, part).wait_recv()

                if s + 1 < reach - 1:

                    @pl.when(bwd_sends(s + 1))
                    def _(s=s, part=part):
                        bwd_copy(s + 1, part).start()

                @pl.when(bwd_needed(s))
                def _(s=s, part=part):
                    core_bwd(s, part, core).start()

        if s == 0:
            hand_on(1)
        if s == 2:
            hand_on(2)
            for way in range(2):
                side_copy(3, way).start()
            for n in range(here):
                source, arrival = row_arrival(n)

                @pl.when(source != me)
                def _(arrival=arrival):
                    arrival.wait_recv()

            @pl.when(is_self)
            def _():
                own_row.wait()

            expert_part(t, True)
        if s == 3:
            expert_part(left, False)
        if s == 4:
            expert_part(right, False)

    hand_on(3)
    for a in range(3):
        for way in range(2):
            half_copy(a, way).wait_recv()
    expert_part(across, False)
    width = result.shape[3]
    for k in far_first:
        n = lax.rem(self_slot + k, here)
        first = pl.multiple_of(n * CAP, CAP)
        for q in range(n_tp):
            result[q, n] = total[pl.ds(first, CAP), q * width : (q + 1) * width].astype(BF16)
    for k in range(here):
        for j in range(n_tp):
            away, copy = back_copy(k, j)

            @pl.when(away)
            def _(copy=copy):
                copy.start()

    @pl.when(is_self)
    def _():
        own_back.start()

    for part in range(2):

        @pl.when(core == 1)
        def _(part=part):
            core_copy(0, part, z, 0).wait_recv()

        for s in range(reach):

            @pl.when(fwd_gets(s))
            def _(s=s, part=part):
                core_fwd(s, part, 1 - core).wait_recv()

            if s < reach - 1:

                @pl.when(bwd_needed(s))
                def _(s=s, part=part):
                    core_bwd(s, part, 1 - core).wait_recv()

    state = (keys_all, values_all, query_t, bias, run_max, run_sum, acc)

    def body(block, carry):
        attend_block(block, False, *state)
        return carry

    for way in range(2):
        part_copy(way, out_first).start()
    lax.fori_loop(0, me, body, 0)
    attend_block(me, True, *state)
    finish_attention(heads, attended, run_sum, acc)
    for way in range(2):
        half_copy(3, way).wait_recv()
    part_copy(2, out_first).start()
    for k in range(1, n_tp):
        head_copy(k).start()
    own_heads.start()

    for a in range(4):
        for way in range(2):
            side_copy(a, way).wait_send()
            half_copy(a, way).wait_send()
    for k in range(here):
        mate, copy = row_copy(k)

        @pl.when(mate != me)
        def _(copy=copy):
            copy.wait_send()

    for part in range(2):

        @pl.when(core == 0)
        def _(part=part):
            core_copy(0, part, z, 0, True).wait_send()

        for s in range(reach):

            @pl.when(fwd_sends(s))
            def _(s=s, part=part):
                fwd_copy(s, part).wait_send()

            @pl.when(fwd_gets(s))
            def _(s=s, part=part):
                core_fwd(s, part, core).wait_send()

            if s < reach - 1:

                @pl.when(bwd_sends(s))
                def _(s=s, part=part):
                    bwd_copy(s, part).wait_send()

                @pl.when(bwd_needed(s))
                def _(s=s, part=part):
                    core_bwd(s, part, core).wait_send()

    for k in range(3):
        part_copy(k, out_first).wait_send()
        part_copy(k, (1 - core) * out_rows).wait_recv()
    own_out[1].wait()
    for k in range(here):
        for j in range(n_tp):
            away, copy = back_copy(k, j)

            @pl.when(away)
            def _(copy=copy):
                copy.wait_send()

    for e in range(n_ep):
        column, away = returns_from(e)
        arrival = remote(
            result.at[0, 0],
            back_ref.at[e],
            back_send.at[0, 0],
            back_recv.at[e],
            {"ep": e, "tp": column},
        )

        @pl.when(away)
        def _(arrival=arrival):
            arrival.wait_recv()

    @pl.when(is_self)
    def _():
        own_back.wait()

    for k in range(1, n_tp):
        source = lax.rem(t + n_tp - k, n_tp)
        head_copy(k).wait_send()
        remote(
            attended.at[pl.ds(0, token_rows)],
            heads_ref.at[source],
            head_send.at[k],
            head_recv.at[k],
            {"tp": source},
        ).wait_recv()
    own_heads.wait()


def combine_kernel(back_ref, routes_ref, weight_ref, heads_ref, out_w_ref, mixer_ref, out_ref):
    slots = back_ref.shape[0]
    span = routes_ref.shape[1]
    expert_col = lax.broadcasted_iota(jnp.int32, (EXPERTS, 1), 0)
    routes = routes_ref[...]
    _, rank = member_and_rank(routes, expert_col)
    total = None
    for j in range(TOP):
        chosen = routes[j : j + 1, :]
        within = jnp.sum(jnp.where(chosen == expert_col, rank, 0.0), axis=0, keepdims=True)
        slot = chosen * CAP + within.astype(jnp.int32)
        at = lax.broadcasted_iota(jnp.int32, (slots, span), 0)
        pick = jnp.where(at == slot, 1.0, 0.0).astype(BF16)
        picked = dot(pick, back_ref[...], (((0,), (0,)), ((), ())))
        term = picked * weight_ref[:, j : j + 1]
        total = term if total is None else total + term
    out_ref[...] = total.astype(BF16)
    projected = None
    for k in range(heads_ref.shape[0]):
        piece = dot(heads_ref[k], out_w_ref[k])
        projected = piece if projected is None else projected + piece
    mixer_ref[...] = projected.astype(BF16)


def on_device(
    n_ep,
    n_tp,
    queries,
    key_rows,
    value_rows,
    query_gain,
    key_gain,
    log_forget,
    out_weight,
    expert_rows,
    expert_gain,
    routes,
    route_weight,
    gate_weight,
    up_weight,
    down_weight,
):
    span, model_width = expert_rows.shape
    here = n_ep // n_tp
    heads = queries.shape[1] // HEAD_SIZE
    width = model_width // n_tp
    n_z = n_ep // CORES
    reach = n_z // 2
    ff_part = gate_weight.shape[2]
    hbm = pl.BlockSpec(memory_space=pltpu.HBM)
    vmem = pl.BlockSpec(memory_space=pltpu.VMEM)
    shape = jax.ShapeDtypeStruct
    big = pltpu.CompilerParams(vmem_limit_bytes=56 * 1024 * 1024)

    send_rows, own_keys, own_values = pl.pallas_call(
        functools.partial(prologue_kernel, n_tp),
        out_shape=(
            shape((here, CAP, model_width), BF16),
            shape((span, HEAD_SIZE), BF16),
            shape((HEAD_SIZE, span), BF16),
        ),
        in_specs=[vmem] * 6,
        out_specs=(vmem,) * 3,
        scratch_shapes=[pltpu.VMEM((span, model_width), BF16)],
        compiler_params=big,
        name="prologue",
    )(
        expert_rows,
        expert_gain.reshape(1, -1),
        routes,
        key_rows,
        value_rows,
        key_gain.reshape(1, -1),
    )

    dma = pltpu.SemaphoreType.DMA
    columns = heads * span
    back_rows, head_rows, out_all = pl.pallas_call(
        functools.partial(layer_kernel, n_ep, n_tp, heads),
        out_shape=(
            shape((n_ep, CAP, width), BF16),
            shape((n_tp, span // n_tp, heads * HEAD_SIZE), BF16),
            shape((n_tp, *out_weight.shape), BF16),
        ),
        in_specs=[hbm] + [vmem] * 5 + [hbm] * 4,
        out_specs=(hbm,) * 3,
        scratch_shapes=[
            pltpu.VMEM((here, CAP, model_width), BF16),
            pltpu.VMEM((here * CAP, model_width), F32),
            pltpu.VMEM((n_tp, here, CAP, width), BF16),
            pltpu.VMEM((span, heads * HEAD_SIZE), BF16),
            pltpu.VMEM((n_ep, span, HEAD_SIZE), BF16),
            pltpu.VMEM((n_ep, HEAD_SIZE, span), BF16),
            pltpu.VMEM((2 * HEAD_SIZE, columns), BF16),
            pltpu.VMEM((n_ep, span, HEAD_SIZE), BF16),
            pltpu.VMEM((1, columns), F32),
            pltpu.VMEM((1, columns), F32),
            pltpu.VMEM((HEAD_SIZE, columns), F32),
            pltpu.VMEM((n_tp, model_width, ff_part), BF16),
            pltpu.VMEM((n_tp, model_width, ff_part), BF16),
            pltpu.VMEM((n_tp, ff_part, model_width), BF16),
            pltpu.VMEM(out_weight.shape, BF16),
            dma((here,)),
            dma((here,)),
            dma((reach, 2)),
            dma((reach, 2)),
            dma((reach - 1, 2)),
            dma((reach - 1, 2)),
            dma((2 * reach, 2)),
            dma((2 * reach, 2)),
            dma((4, 2)),
            dma((4, 2)),
            dma((4, 2)),
            dma((4, 2)),
            dma((3,)),
            dma((3,)),
            dma((here, n_tp)),
            dma((n_ep,)),
            dma((n_tp,)),
            dma((n_tp,)),
            dma((5,)),
        ],
        compiler_params=pltpu.CompilerParams(
            collective_id=0, has_side_effects=True, vmem_limit_bytes=60 * 1024 * 1024
        ),
        name="layer",
    )(
        send_rows,
        own_keys,
        own_values,
        queries,
        query_gain.reshape(1, -1),
        log_forget,
        gate_weight.reshape(model_width, ff_part),
        up_weight.reshape(model_width, ff_part),
        down_weight.reshape(ff_part, model_width),
        out_weight,
    )

    mixer_out, expert_out = pl.pallas_call(
        combine_kernel,
        out_shape=(
            shape((span // n_tp, model_width), BF16),
            shape((span, width), BF16),
        ),
        in_specs=[vmem] * 5,
        out_specs=(vmem, vmem),
        compiler_params=big,
        name="combine",
    )(back_rows.reshape(n_ep * CAP, width), routes, route_weight.T, head_rows, out_all)
    return (mixer_out, expert_out)


def solution(mesh):
    in_specs = (
        P(("grp", "ep"), "tp"),
        P(("grp", "ep"), "tp"),
        P(("grp", "ep"), "tp"),
        P(),
        P(),
        P("tp", "grp"),
        P("tp", None),
        P(("grp", "ep"), None),
        P(),
        P(None, ("grp", "ep")),
        P(None, ("grp", "ep")),
        P("ep", None, "tp"),
        P("ep", None, "tp"),
        P("ep", "tp", None),
    )
    out_specs = (P(("grp", "ep", "tp"), None), P(("grp", "ep"), "tp"))
    return jax.shard_map(
        functools.partial(on_device, mesh.shape["ep"], mesh.shape["tp"]),
        mesh=mesh,
        in_specs=in_specs,
        out_specs=out_specs,
        check_vma=False,
    )
```

time: 286 us -> 234 us (0.82)
  Pallas kernels: 281 us -> 230 us
    pallas_call x3 -> x1, Pallas kernels: 268 us -> 217 us  [on_device(): pl.pallas_call(functools.partial(layer_kernel, n_ep, n_tp, heads), out_sh...]
where the time goes in v3:
time: 234 us; the launch traced here: 231 us
  Pallas kernels  230 us (98%)
    pallas_call x1, Pallas kernels, on_device(): pl.pallas_call(functools.partial(layer_kernel, n_ep, n_tp, heads), out_sh...  217 us
    pallas_call x1, Pallas kernels, on_device(): pl.pallas_call(functools.partial(prologue_kernel, n_tp), out_shape=(shape...  6.55 us
    pallas_call x1, Pallas kernels, on_device(): pl.pallas_call(combine_kernel, out_shape=(shape((span // n_tp, model_widt...  6.28 us

profile of v3, /device:TPU:46, one launch (start us, length us, event | category | flops | bytes accessed | tf_op | source)
XLA Modules:
  0.0 231.1 jit_solution(4531974378272155072)
XLA Ops:
  0.6 6.5 %prologue.1 = (bf16[8,48,2048]{2,1,0:T(8,128)(2,1)}, bf16[512,128]{1,0:T(8,128)(2,1)}, bf16[128,512]{1,0:T(8,128)(2,1)}) custom-call(bf16[512,2048]{1,0:T(8,128)(2,1)} %rows_ref.1, f32[1,2048]{1,0:T(1,128)} %bitcast.13, s32[2,512]{1,0:T(2,128)} %routes_ref.3, bf16[512,128]{1,0:T(8,128)(2,1)} %key_ref.1, bf16[512,128]{1,0:T(8,128)(2,1)} %value_ref.1, ...), custom_call_target="tpu_custom_call" | custom-call | tf_op jit(solution)/shard_map/prologue/pallas_call | solution.py:712
  7.2 0.0 copy-start
  7.2 216.7 %layer.1 = (bf16[32,48,512]{2,1,0:T(8,128)(2,1)}, bf16[4,128,256]{2,1,0:T(8,128)(2,1)}, bf16[4,256,2048]{2,1,0:T(8,128)(2,1)}) custom-call(bf16[8,48,2048]{2,1,0:T(8,128)(2,1)} %get-tuple-element.8.send_ref, bf16[512,128]{1,0:T(8,128)(2,1)} %get-tuple-element.9.key_ref, bf16[128,512]{1,0:T(8,128)(2,1)} %get-tuple-element.10.value_ref, ...), custom_call_target="tpu_custom_call" | custom-call | tf_op jit(solution)/shard_map/layer/pallas_call | solution.py:735
  223.9 0.0 copy-done
  223.9 0.9 copy.16
  224.8 6.3 %combine.1 = (bf16[128,2048]{1,0:T(8,128)(2,1)}, bf16[512,512]{1,0:T(8,128)(2,1)}) custom-call(bf16[1536,512]{1,0:T(8,128)(2,1)} %bitcast.8, s32[2,512]{1,0:T(2,128)} %routes_ref.3, f32[512,2]{1,0:T(8,128)} %bitcast.12, bf16[4,128,256]{2,1,0:T(8,128)(2,1)} %get-tuple-element.12.heads_ref, bf16[4,256,2048]{2,1,0:T(8,128)(2,1)} %get-tuple-element.13.out_w_ref), custom_call_target="tpu_custom_call" | custom-call | tf_op jit(solution)/shard_map/combine/pallas_call | solution.py:797
Async XLA Ops:
  7.2 216.7 %copy-start = (f32[2,512]{1,0:T(2,128)S(1)}, f32[2,512]{1,0:T(2,128)}, u32[]{:S(2)}) copy-start(f32[2,512]{1,0:T(2,128)} %param.24) | copy-start | bytes 12292

commit v4 on v3

--- a/solution.py
+++ b/solution.py
@@ -30,34 +30,16 @@
 
 def member_and_rank(routes, expert_col):
     tokens = routes.shape[1]
-    count = expert_col.shape[0]
     named = jnp.logical_or(routes[0:1, :] == expert_col, routes[1:2, :] == expert_col)
     member = jnp.where(named, 1.0, 0.0).astype(F32)
     before = lax.broadcasted_iota(jnp.int32, (tokens, tokens), 0)
     after = lax.broadcasted_iota(jnp.int32, (tokens, tokens), 1)
     earlier = jnp.where(before < after, 1.0, 0.0).astype(BF16)
-    del count
     return member, dot(member.astype(BF16), earlier)
 
 
-def prologue_kernel(
-    n_tp,
-    rows_ref,
-    gain_ref,
-    routes_ref,
-    key_ref,
-    value_ref,
-    key_gain_ref,
-    send_ref,
-    own_key_ref,
-    own_value_ref,
-    normed,
-):
+def gather_rows(n_tp, offset, rows_ref, gain_ref, routes_ref, send, normed):
     span = rows_ref.shape[0]
-    me, t = lax.axis_index("ep"), lax.axis_index("tp")
-    offset = lax.rem(t + (n_tp - 1) * me, n_tp)
-    own_key_ref[...] = row_norm(key_ref[...], key_gain_ref[...]).astype(BF16)
-    own_value_ref[...] = value_ref[...].astype(F32).T.astype(BF16)
     step = 64
     for first in range(0, span, step):
         normed[first : first + step, :] = row_norm(
@@ -70,7 +52,20 @@
     slot = lax.broadcasted_iota(jnp.int32, (CAP, span), 0).astype(F32)
     for m in range(here):
         pick = jnp.where(place[m : m + 1, :] == slot, 1.0, 0.0).astype(BF16)
-        send_ref[m] = dot(pick, normed[...]).astype(BF16)
+        send[m] = dot(pick, normed[...]).astype(BF16)
+
+
+def token_columns(routes, weights):
+    expert_col = lax.broadcasted_iota(jnp.int32, (EXPERTS, 1), 0)
+    _, rank = member_and_rank(routes, expert_col)
+    rows = []
+    for j in range(TOP):
+        chosen = routes[j : j + 1, :]
+        within = jnp.sum(jnp.where(chosen == expert_col, rank, 0.0), axis=0, keepdims=True)
+        rows.append((chosen * CAP).astype(F32) + within)
+    rows.append(weights)
+    rows.append(jnp.zeros((8 - 2 * TOP, routes.shape[1]), F32))
+    return jnp.concatenate(rows, axis=0).T
 
 
 def split_three(value):
@@ -160,9 +155,13 @@
     n_ep,
     n_tp,
     heads,
-    send_ref,
-    key_ref,
-    value_ref,
+    rows_ref,
+    rows_gain_ref,
+    routes_ref,
+    route_weight_ref,
+    raw_key_ref,
+    raw_value_ref,
+    key_gain_ref,
     query_ref,
     query_gain_ref,
     forget_ref,
@@ -170,9 +169,17 @@
     up_ref,
     down_ref,
     out_ref,
+    mixer_ref,
+    expert_ref,
+    send_ref,
+    normed,
+    columns_ref,
+    picks,
     back_ref,
     heads_ref,
     out_all,
+    key_ref,
+    value_ref,
     rows_all,
     total,
     result,
@@ -187,7 +194,6 @@
     gate_all,
     up_all,
     down_all,
-    out_own,
     row_send,
     row_recv,
     fwd_send,
@@ -296,13 +302,7 @@
         pltpu.make_async_copy(src, full.at[t], local.at[a])
         for a, (src, full) in enumerate(weights)
     ]
-    own_row = pltpu.make_async_copy(
-        send_ref.at[self_slot], rows_all.at[self_slot], local.at[3]
-    )
-    own_out = (
-        pltpu.make_async_copy(out_ref, out_own, local.at[4]),
-        pltpu.make_async_copy(out_own, out_all.at[t], local.at[4]),
-    )
+    own_out = pltpu.make_async_copy(out_ref, out_all.at[t], local.at[3])
 
     def row_copy(k):
         m = lax.rem(self_slot + k, here)
@@ -381,8 +381,6 @@
             {"ep": target, "tp": q},
         )
 
-    own_back = pltpu.make_async_copy(result.at[t, self_slot], back_ref.at[me], local.at[3])
-
     token_rows = attended.shape[0] // n_tp
 
     def head_copy(k):
@@ -395,12 +393,6 @@
             head_recv.at[k],
             {"tp": q},
         )
-
-    own_heads = pltpu.make_async_copy(
-        attended.at[pl.ds(pl.multiple_of(t * token_rows, token_rows), token_rows)],
-        heads_ref.at[t],
-        local.at[0],
-    )
 
     def expert_part(p, first):
         rows = rows_all[...].reshape(here * CAP, rows_all.shape[2])
@@ -420,6 +412,29 @@
         for way in range(2):
             side_copy(a, way).start()
 
+    key_ref[...] = row_norm(raw_key_ref[...], key_gain_ref[...]).astype(BF16)
+    value_ref[...] = raw_value_ref[...].astype(F32).T.astype(BF16)
+    keys_all[me] = key_ref[...]
+    values_all[me] = value_ref[...]
+    for copy in own:
+        copy.start()
+    own_out.start()
+    for part in range(2):
+
+        @pl.when(fwd_sends(0))
+        def _(part=part):
+            fwd_copy(0, part).start()
+
+        @pl.when(bwd_sends(0))
+        def _(part=part):
+            bwd_copy(0, part).start()
+
+        @pl.when(core == 0)
+        def _(part=part):
+            core_copy(0, part, z, 0, True).start()
+
+    gather_rows(n_tp, offset, rows_ref, rows_gain_ref, routes_ref, send_ref, normed)
+    columns_ref[...] = token_columns(routes_ref[...], route_weight_ref[...])
     for k in far_first:
         mate, copy = row_copy(k)
 
@@ -427,35 +442,13 @@
         def _(copy=copy):
             copy.start()
 
-    for part in range(2):
-
-        @pl.when(fwd_sends(0))
-        def _(part=part):
-            fwd_copy(0, part).start()
-
-        @pl.when(bwd_sends(0))
-        def _(part=part):
-            bwd_copy(0, part).start()
-
-        @pl.when(core == 0)
-        def _(part=part):
-            core_copy(0, part, z, 0, True).start()
-
-    for copy in own:
-        copy.start()
-    own_out[0].start()
-
     @pl.when(is_self)
     def _():
-        own_row.start()
-
-    keys_all[me] = key_ref[...]
-    values_all[me] = value_ref[...]
+        rows_all[self_slot] = send_ref[self_slot]
+
     prepare_attention(
         heads, me + 1, query_ref, query_gain_ref, forget_ref, query_t, bias, run_max, run_sum, acc
     )
-    own_out[0].wait()
-    own_out[1].start()
     for copy in own:
         copy.wait()
 
@@ -499,6 +492,7 @@
             hand_on(2)
             for way in range(2):
                 side_copy(3, way).start()
+        if s == 3:
             for n in range(here):
                 source, arrival = row_arrival(n)
 
@@ -506,39 +500,37 @@
                 def _(arrival=arrival):
                     arrival.wait_recv()
 
+            expert_part(t, True)
+        if s == 4:
+            expert_part(left, False)
+        if s == 5:
+            expert_part(right, False)
+        if s == 6:
+            for a in range(3):
+                for way in range(2):
+                    half_copy(a, way).wait_recv()
+            expert_part(across, False)
+            width = result.shape[3]
+            for k in far_first:
+                n = lax.rem(self_slot + k, here)
+                first = pl.multiple_of(n * CAP, CAP)
+                for q in range(n_tp):
+                    result[q, n] = total[pl.ds(first, CAP), q * width : (q + 1) * width].astype(
+                        BF16
+                    )
+            for k in range(here):
+                for j in range(n_tp):
+                    away, copy = back_copy(k, j)
+
+                    @pl.when(away)
+                    def _(copy=copy):
+                        copy.start()
+
             @pl.when(is_self)
             def _():
-                own_row.wait()
-
-            expert_part(t, True)
-        if s == 3:
-            expert_part(left, False)
-        if s == 4:
-            expert_part(right, False)
+                back_ref[me] = result[t, self_slot]
 
     hand_on(3)
-    for a in range(3):
-        for way in range(2):
-            half_copy(a, way).wait_recv()
-    expert_part(across, False)
-    width = result.shape[3]
-    for k in far_first:
-        n = lax.rem(self_slot + k, here)
-        first = pl.multiple_of(n * CAP, CAP)
-        for q in range(n_tp):
-            result[q, n] = total[pl.ds(first, CAP), q * width : (q + 1) * width].astype(BF16)
-    for k in range(here):
-        for j in range(n_tp):
-            away, copy = back_copy(k, j)
-
-            @pl.when(away)
-            def _(copy=copy):
-                copy.start()
-
-    @pl.when(is_self)
-    def _():
-        own_back.start()
-
     for part in range(2):
 
         @pl.when(core == 1)
@@ -573,7 +565,11 @@
     part_copy(2, out_first).start()
     for k in range(1, n_tp):
         head_copy(k).start()
-    own_heads.start()
+    own_first = pl.multiple_of(t * token_rows, token_rows)
+    heads_ref[t] = attended[pl.ds(own_first, token_rows), :]
+    slot = lax.broadcasted_iota(jnp.int32, (8, n_ep * CAP), 1).astype(F32)[:1]
+    for j in range(TOP):
+        picks[j] = jnp.where(columns_ref[:, j : j + 1] == slot, 1.0, 0.0).astype(BF16)
 
     for a in range(4):
         for way in range(2):
@@ -615,33 +611,7 @@
     for k in range(3):
         part_copy(k, out_first).wait_send()
         part_copy(k, (1 - core) * out_rows).wait_recv()
-    own_out[1].wait()
-    for k in range(here):
-        for j in range(n_tp):
-            away, copy = back_copy(k, j)
-
-            @pl.when(away)
-            def _(copy=copy):
-                copy.wait_send()
-
-    for e in range(n_ep):
-        column, away = returns_from(e)
-        arrival = remote(
-            result.at[0, 0],
-            back_ref.at[e],
-            back_send.at[0, 0],
-            back_recv.at[e],
-            {"ep": e, "tp": column},
-        )
-
-        @pl.when(away)
-        def _(arrival=arrival):
-            arrival.wait_recv()
-
-    @pl.when(is_self)
-    def _():
-        own_back.wait()
-
+    own_out.wait()
     for k in range(1, n_tp):
         source = lax.rem(t + n_tp - k, n_tp)
         head_copy(k).wait_send()
@@ -652,31 +622,40 @@
             head_recv.at[k],
             {"tp": source},
         ).wait_recv()
-    own_heads.wait()
-
-
-def combine_kernel(back_ref, routes_ref, weight_ref, heads_ref, out_w_ref, mixer_ref, out_ref):
-    slots = back_ref.shape[0]
-    span = routes_ref.shape[1]
-    expert_col = lax.broadcasted_iota(jnp.int32, (EXPERTS, 1), 0)
-    routes = routes_ref[...]
-    _, rank = member_and_rank(routes, expert_col)
-    total = None
-    for j in range(TOP):
-        chosen = routes[j : j + 1, :]
-        within = jnp.sum(jnp.where(chosen == expert_col, rank, 0.0), axis=0, keepdims=True)
-        slot = chosen * CAP + within.astype(jnp.int32)
-        at = lax.broadcasted_iota(jnp.int32, (slots, span), 0)
-        pick = jnp.where(at == slot, 1.0, 0.0).astype(BF16)
-        picked = dot(pick, back_ref[...], (((0,), (0,)), ((), ())))
-        term = picked * weight_ref[:, j : j + 1]
-        total = term if total is None else total + term
-    out_ref[...] = total.astype(BF16)
     projected = None
-    for k in range(heads_ref.shape[0]):
-        piece = dot(heads_ref[k], out_w_ref[k])
+    for k in range(n_tp):
+        piece = dot(heads_ref[k], out_all[k])
         projected = piece if projected is None else projected + piece
     mixer_ref[...] = projected.astype(BF16)
+
+    for k in range(here):
+        for j in range(n_tp):
+            away, copy = back_copy(k, j)
+
+            @pl.when(away)
+            def _(copy=copy):
+                copy.wait_send()
+
+    for e in range(n_ep):
+        column, away = returns_from(e)
+        arrival = remote(
+            result.at[0, 0],
+            back_ref.at[e],
+            back_send.at[0, 0],
+            back_recv.at[e],
+            {"ep": e, "tp": column},
+        )
+
+        @pl.when(away)
+        def _(arrival=arrival):
+            arrival.wait_recv()
+
+    expert_out = None
+    for j in range(TOP):
+        picked = dot(picks[j], back_ref[...].reshape(n_ep * CAP, back_ref.shape[2]))
+        term = picked * columns_ref[:, TOP + j : TOP + j + 1]
+        expert_out = term if expert_out is None else expert_out + term
+    expert_ref[...] = expert_out.astype(BF16)
 
 
 def on_device(
@@ -707,41 +686,26 @@
     hbm = pl.BlockSpec(memory_space=pltpu.HBM)
     vmem = pl.BlockSpec(memory_space=pltpu.VMEM)
     shape = jax.ShapeDtypeStruct
-    big = pltpu.CompilerParams(vmem_limit_bytes=56 * 1024 * 1024)
-
-    send_rows, own_keys, own_values = pl.pallas_call(
-        functools.partial(prologue_kernel, n_tp),
-        out_shape=(
-            shape((here, CAP, model_width), BF16),
-            shape((span, HEAD_SIZE), BF16),
-            shape((HEAD_SIZE, span), BF16),
-        ),
-        in_specs=[vmem] * 6,
-        out_specs=(vmem,) * 3,
-        scratch_shapes=[pltpu.VMEM((span, model_width), BF16)],
-        compiler_params=big,
-        name="prologue",
-    )(
-        expert_rows,
-        expert_gain.reshape(1, -1),
-        routes,
-        key_rows,
-        value_rows,
-        key_gain.reshape(1, -1),
-    )
-
     dma = pltpu.SemaphoreType.DMA
     columns = heads * span
-    back_rows, head_rows, out_all = pl.pallas_call(
+    return pl.pallas_call(
         functools.partial(layer_kernel, n_ep, n_tp, heads),
         out_shape=(
-            shape((n_ep, CAP, width), BF16),
-            shape((n_tp, span // n_tp, heads * HEAD_SIZE), BF16),
-            shape((n_tp, *out_weight.shape), BF16),
+            shape((span // n_tp, model_width), BF16),
+            shape((span, width), BF16),
         ),
-        in_specs=[hbm] + [vmem] * 5 + [hbm] * 4,
-        out_specs=(hbm,) * 3,
+        in_specs=[vmem] * 10 + [hbm] * 4,
+        out_specs=(vmem, vmem),
         scratch_shapes=[
+            pltpu.VMEM((here, CAP, model_width), BF16),
+            pltpu.VMEM((span, model_width), BF16),
+            pltpu.VMEM((span, 8), F32),
+            pltpu.VMEM((TOP, span, n_ep * CAP), BF16),
+            pltpu.VMEM((n_ep, CAP, width), BF16),
+            pltpu.VMEM((n_tp, span // n_tp, heads * HEAD_SIZE), BF16),
+            pltpu.VMEM((n_tp, *out_weight.shape), BF16),
+            pltpu.VMEM((span, HEAD_SIZE), BF16),
+            pltpu.VMEM((HEAD_SIZE, span), BF16),
             pltpu.VMEM((here, CAP, model_width), BF16),
             pltpu.VMEM((here * CAP, model_width), F32),
             pltpu.VMEM((n_tp, here, CAP, width), BF16),
@@ -756,7 +720,6 @@
             pltpu.VMEM((n_tp, model_width, ff_part), BF16),
             pltpu.VMEM((n_tp, model_width, ff_part), BF16),
             pltpu.VMEM((n_tp, ff_part, model_width), BF16),
-            pltpu.VMEM(out_weight.shape, BF16),
             dma((here,)),
             dma((here,)),
             dma((reach, 2)),
@@ -775,16 +738,20 @@
             dma((n_ep,)),
             dma((n_tp,)),
             dma((n_tp,)),
-            dma((5,)),
+            dma((4,)),
         ],
         compiler_params=pltpu.CompilerParams(
             collective_id=0, has_side_effects=True, vmem_limit_bytes=60 * 1024 * 1024
         ),
         name="layer",
     )(
-        send_rows,
-        own_keys,
-        own_values,
+        expert_rows,
+        expert_gain.reshape(1, -1),
+        routes,
+        route_weight,
+        key_rows,
+        value_rows,
+        key_gain.reshape(1, -1),
         queries,
         query_gain.reshape(1, -1),
         log_forget,
@@ -793,19 +760,6 @@
         down_weight.reshape(ff_part, model_width),
         out_weight,
     )
-
-    mixer_out, expert_out = pl.pallas_call(
-        combine_kernel,
-        out_shape=(
-            shape((span // n_tp, model_width), BF16),
-            shape((span, width), BF16),
-        ),
-        in_specs=[vmem] * 5,
-        out_specs=(vmem, vmem),
-        compiler_params=big,
-        name="combine",
-    )(back_rows.reshape(n_ep * CAP, width), routes, route_weight.T, head_rows, out_all)
-    return (mixer_out, expert_out)
 
 
 def solution(mesh):

time: 234 us -> 221 us (0.944)
  Pallas kernels: 230 us -> 214 us
  local copies, waits for them, and re-layouts: 0.87 us -> 3.75 us
    pallas_call x2 -> x0, Pallas kernels: 12.8 us -> none  [the longest x1 6.55 us: on_device(): pl.pallas_call(functools.partial(prologue_kernel, n_tp), out_shape=(shape...]
    unnamed x3 -> x2, local copies, waits for them, and re-layouts: 0.87 us -> 3.75 us
    pallas_call x1, Pallas kernels: 217 us -> 214 us  [on_device(): pl.pallas_call(functools.partial(layer_kernel, n_ep, n_tp, heads), out_sh...]
where the time goes in v4:
time: 221 us; the launch traced here: 218 us
  Pallas kernels  214 us (97%)
  local copies, waits for them, and re-layouts  3.75 us (2%)
    pallas_call x1, Pallas kernels, on_device(): pl.pallas_call(functools.partial(layer_kernel, n_ep, n_tp, heads), out_sh...  214 us

profile of v4, /device:TPU:46, one launch (start us, length us, event | category | flops | bytes accessed | tf_op | source)
XLA Modules:
  0.0 218.4 jit_solution(3722763906299520661)
XLA Ops:
  0.6 214.0 %layer.1 = (bf16[128,2048]{1,0:T(8,128)(2,1)}, bf16[512,512]{1,0:T(8,128)(2,1)}) custom-call(bf16[512,2048]{1,0:T(8,128)(2,1)} %rows_ref.1, f32[1,2048]{1,0:T(1,128)} %bitcast.9, s32[2,512]{1,0:T(2,128)} %routes_ref.1, f32[2,512]{1,0:T(2,128)} %route_weight_ref.1, bf16[512,128]{1,0:T(8,128)(2,1)} %raw_key_ref.1, bf16[512,128]{1,0:T(8,128)(2,1)} %raw_value_ref.1, ...), custom_call_target="tpu_custom_call" | custom-call | tf_op jit(solution)/shard_map/layer/pallas_call | solution.py:691
  214.7 1.9 copy.18
  216.6 1.9 copy.19

commit v5 on v4

--- a/solution.py
+++ b/solution.py
@@ -394,12 +394,16 @@
             {"tp": q},
         )
 
-    def expert_part(p, first):
+    width = result.shape[3]
+
+    def expert_hidden(p):
         rows = rows_all[...].reshape(here * CAP, rows_all.shape[2])
         gate = dot(rows, gate_all[p])
         up = dot(rows, up_all[p])
-        hidden = (gate / (1.0 + jnp.exp(-gate)) * up).astype(BF16)
-        width = result.shape[3]
+        return (gate / (1.0 + jnp.exp(-gate)) * up).astype(BF16)
+
+    def expert_part(p, first):
+        hidden = expert_hidden(p)
         for q in range(n_tp):
             cols = slice(q * width, (q + 1) * width)
             piece = dot(hidden, down_all[p, :, cols]).astype(BF16).astype(F32)
@@ -407,6 +411,31 @@
                 total[:, cols] = piece
             else:
                 total[:, cols] += piece
+
+    def send_back(j):
+        for k in range(here):
+            away, copy = back_copy(k, j)
+
+            @pl.when(away)
+            def _(copy=copy):
+                copy.start()
+
+    def last_part(p):
+        hidden = expert_hidden(p)
+        for j in range(n_tp):
+            q = lax.rem(t + j, n_tp)
+            cols = pl.ds(pl.multiple_of(q * width, width), width)
+            piece = dot(hidden, down_all[p, :, cols]).astype(BF16).astype(F32)
+            done = (total[:, cols] + piece).astype(BF16)
+            result[q] = done.reshape(here, CAP, width)
+            if j > 0:
+                send_back(j - 1)
+
+        @pl.when(is_self)
+        def _():
+            back_ref[me] = result[t, self_slot]
+
+        send_back(n_tp - 1)
 
     for a in range(3):
         for way in range(2):
@@ -509,26 +538,7 @@
             for a in range(3):
                 for way in range(2):
                     half_copy(a, way).wait_recv()
-            expert_part(across, False)
-            width = result.shape[3]
-            for k in far_first:
-                n = lax.rem(self_slot + k, here)
-                first = pl.multiple_of(n * CAP, CAP)
-                for q in range(n_tp):
-                    result[q, n] = total[pl.ds(first, CAP), q * width : (q + 1) * width].astype(
-                        BF16
-                    )
-            for k in range(here):
-                for j in range(n_tp):
-                    away, copy = back_copy(k, j)
-
-                    @pl.when(away)
-                    def _(copy=copy):
-                        copy.start()
-
-            @pl.when(is_self)
-            def _():
-                back_ref[me] = result[t, self_slot]
+            last_part(across)
 
     hand_on(3)
     for part in range(2):
@@ -656,6 +666,11 @@
         term = picked * columns_ref[:, TOP + j : TOP + j + 1]
         expert_out = term if expert_out is None else expert_out + term
     expert_ref[...] = expert_out.astype(BF16)
+
+
+def settle_kernel(mixer_in, expert_in, mixer_ref, expert_ref):
+    mixer_ref[...] = mixer_in[...]
+    expert_ref[...] = expert_in[...]
 
 
 def on_device(
@@ -688,7 +703,7 @@
     shape = jax.ShapeDtypeStruct
     dma = pltpu.SemaphoreType.DMA
     columns = heads * span
-    return pl.pallas_call(
+    mixer_out, expert_out = pl.pallas_call(
         functools.partial(layer_kernel, n_ep, n_tp, heads),
         out_shape=(
             shape((span // n_tp, model_width), BF16),
@@ -760,6 +775,20 @@
         down_weight.reshape(ff_part, model_width),
         out_weight,
     )
+    steps = 2
+    mixer_block = pl.BlockSpec((span // n_tp // steps, model_width), lambda i: (i, 0))
+    expert_block = pl.BlockSpec((span // steps, width), lambda i: (i, 0))
+    return pl.pallas_call(
+        settle_kernel,
+        grid=(steps,),
+        out_shape=(
+            shape((span // n_tp, model_width), BF16),
+            shape((span, width), BF16),
+        ),
+        in_specs=[mixer_block, expert_block],
+        out_specs=(mixer_block, expert_block),
+        name="settle",
+    )(mixer_out, expert_out)
 
 
 def solution(mesh):

time: 221 us -> 224 us (1.014)
  the two profiles are of different devices: /device:TPU:46 before, /device:TPU:45 now
where the time goes in v5:
time: 224 us; the launch traced here: 223 us
  Pallas kernels  223 us (100%)
    pallas_call x1, Pallas kernels, on_device(): pl.pallas_call(functools.partial(layer_kernel, n_ep, n_tp, heads), out_sh...  221 us

profile of v5, /device:TPU:45, one launch (start us, length us, event | category | flops | bytes accessed | tf_op | source)
XLA Modules:
  0.0 223.4 jit_solution(16252084372861987159)
XLA Ops:
  0.6 220.7 %layer.1 = (bf16[128,2048]{1,0:T(8,128)(2,1)}, bf16[512,512]{1,0:T(8,128)(2,1)}) custom-call(bf16[512,2048]{1,0:T(8,128)(2,1)} %rows_ref.1, f32[1,2048]{1,0:T(1,128)} %bitcast.9, s32[2,512]{1,0:T(2,128)} %routes_ref.1, f32[2,512]{1,0:T(2,128)} %route_weight_ref.1, bf16[512,128]{1,0:T(8,128)(2,1)} %raw_key_ref.1, bf16[512,128]{1,0:T(8,128)(2,1)} %raw_value_ref.1, ...), custom_call_target="tpu_custom_call" | custom-call | tf_op jit(solution)/shard_map/layer/pallas_call | solution.py:706
  221.4 2.0 settle.1

commit v6 on v4

--- a/solution.py
+++ b/solution.py
@@ -658,6 +658,11 @@
     expert_ref[...] = expert_out.astype(BF16)
 
 
+def settle_kernel(mixer_in, expert_in, mixer_ref, expert_ref):
+    mixer_ref[...] = mixer_in[...]
+    expert_ref[...] = expert_in[...]
+
+
 def on_device(
     n_ep,
     n_tp,
@@ -688,7 +693,7 @@
     shape = jax.ShapeDtypeStruct
     dma = pltpu.SemaphoreType.DMA
     columns = heads * span
-    return pl.pallas_call(
+    mixer_out, expert_out = pl.pallas_call(
         functools.partial(layer_kernel, n_ep, n_tp, heads),
         out_shape=(
             shape((span // n_tp, model_width), BF16),
@@ -760,6 +765,20 @@
         down_weight.reshape(ff_part, model_width),
         out_weight,
     )
+    steps = 2
+    mixer_block = pl.BlockSpec((span // n_tp // steps, model_width), lambda i: (i, 0))
+    expert_block = pl.BlockSpec((span // steps, width), lambda i: (i, 0))
+    return pl.pallas_call(
+        settle_kernel,
+        grid=(steps,),
+        out_shape=(
+            shape((span // n_tp, model_width), BF16),
+            shape((span, width), BF16),
+        ),
+        in_specs=[mixer_block, expert_block],
+        out_specs=(mixer_block, expert_block),
+        name="settle",
+    )(mixer_out, expert_out)
 
 
 def solution(mesh):

time: 221 us -> 220 us (level)
  local copies, waits for them, and re-layouts: 3.75 us -> 0 us
    unnamed x2 -> x0, local copies, waits for them, and re-layouts: 3.75 us -> none
where the time goes in v6:
time: 220 us; the launch traced here: 217 us
  Pallas kernels  216 us (98%)
    pallas_call x1, Pallas kernels, on_device(): pl.pallas_call(functools.partial(layer_kernel, n_ep, n_tp, heads), out_sh...  214 us

profile of v6, /device:TPU:46, one launch (start us, length us, event | category | flops | bytes accessed | tf_op | source)
XLA Modules:
  0.0 216.7 jit_solution(11181143614619303977)
XLA Ops:
  0.6 214.0 %layer.1 = (bf16[128,2048]{1,0:T(8,128)(2,1)}, bf16[512,512]{1,0:T(8,128)(2,1)}) custom-call(bf16[512,2048]{1,0:T(8,128)(2,1)} %rows_ref.1, f32[1,2048]{1,0:T(1,128)} %bitcast.9, s32[2,512]{1,0:T(2,128)} %routes_ref.1, f32[2,512]{1,0:T(2,128)} %route_weight_ref.1, bf16[512,128]{1,0:T(8,128)(2,1)} %raw_key_ref.1, bf16[512,128]{1,0:T(8,128)(2,1)} %raw_value_ref.1, ...), custom_call_target="tpu_custom_call" | custom-call | tf_op jit(solution)/shard_map/layer/pallas_call | solution.py:696
  214.7 2.0 settle.1
